TPU v7x, 512 devices: a whole 4x4x16 slice. The times are simulated.
512 devices in a mesh: sp: 32 (over z, core), tp: 16 (over y, x).
Axes of the slice: x: 4, y: 4, z: 16, core: 2. Of those that a mesh axis runs over, the one named last changes fastest.
Arguments:
- moe_input: bfloat16 [5632, 2048], P('sp'), may hold values from -6 to 6
- cotangent: bfloat16 [5632, 2048], P('sp'), may hold values from -6 to 6
- route_ids: int32 [5632, 2], P('sp'), may hold values from 0 to 31, all different within a row; in each aligned block of 176 rows (0 to 175, 176 to 351, ...) at most 22 rows name the same one
- route_weights: float32 [5632, 2], P('sp'), may hold values from 0.25 to 1.5
- expert_gate: bfloat16 [32, 2048, 1024], P('sp', None, 'tp'), may hold values from -0.125 to 0.125
- expert_up: bfloat16 [32, 2048, 1024], P('sp', None, 'tp'), may hold values from -0.125 to 0.125
- expert_down: bfloat16 [32, 1024, 2048], P('sp', 'tp'), may hold values from -0.1875 to 0.1875
- out_proj: bfloat16 [2048, 2048], P('tp'), may hold values from -0.125 to 0.125
- gate_b: bfloat16 [5632, 2048], P('sp', 'tp'), may hold values from -6 to 6
- gate_c: bfloat16 [5632, 2048], P('sp', 'tp'), may hold values from -6 to 6
- conv_in: bfloat16 [5632, 2048], P('sp', 'tp'), may hold values from -6 to 6
- taps: float32 [3, 2048], P(None, 'tp'), may hold values from -4 to 4
Outputs:
- grad_expert_gate: float32 [32, 2048, 1024], P('sp', None, 'tp')
- grad_expert_up: float32 [32, 2048, 1024], P('sp', None, 'tp')
- grad_expert_down: float32 [32, 1024, 2048], P('sp', 'tp')
- grad_out_proj: float32 [2048, 2048], P('tp', 'sp')
- grad_gate_b: bfloat16 [5632, 2048], P('sp', 'tp')
- grad_gate_c: bfloat16 [5632, 2048], P('sp', 'tp')
- grad_conv_in: bfloat16 [5632, 2048], P('sp', 'tp')
Inputs may be any that keep to these rules, and one draw needn't show every extreme that they name: `route_ids`: in the 176 rows of each index of sp, each row names 2 different experts, no expert is named by more than 22 rows, a bound that some block reaches.
All inputs are finite; a program needn't handle non-finite values.
Results may differ from a plain program's by a relative error of at most 0.033.
Values may be sent and summed in bfloat16 or wider, within the bound.
A program may use at most 64 MiB of HBM per device.

v0:
```python
import jax
import jax.numpy as jnp
from jax import lax
from jax.sharding import PartitionSpec as P

EXP_DEV = 1


def sent_together(arrays, axis, split_dim, concat_dim, along):
    widths = [a.shape[along] for a in arrays]
    both = jnp.concatenate(arrays, axis=along)
    out = lax.all_to_all(both, axis, split_axis=split_dim, concat_axis=concat_dim, tiled=True)
    return tuple(jnp.split(out, [sum(widths[:k]) for k in range(1, len(widths))], axis=along))


def side_by_side(arrays, axis, dim, along):
    ends, at = ([], 0)
    for a in arrays[:-1]:
        at += a.shape[along]
        ends.append(at)
    both = jnp.concatenate(arrays, axis=along)
    return tuple(jnp.split(lax.all_gather(both, axis, axis=dim, tiled=True), ends, axis=along))


def split_up(x, dim, devices):
    dims = x.shape
    tiles = x.reshape(*dims[:dim], devices, dims[dim] // devices, *dims[dim + 1 :])
    return jnp.moveaxis(tiles, dim, 0)


def sum_at_owner(x, axis, dim):
    devices = lax.axis_size(axis)
    tiles = lax.all_to_all(split_up(x, dim, devices), axis, 0, 0, tiled=True)
    return jnp.sum(tiles.astype(jnp.float32), axis=0)


def copy_for_each(x, axis):
    devices = lax.axis_size(axis)
    return lax.all_to_all(jnp.broadcast_to(x[None], (devices, *x.shape)), axis, 0, 0, tiled=True)


def in_order(tiles, dim):
    tiles = jnp.moveaxis(tiles, 0, dim)
    dims = tiles.shape
    return tiles.reshape(*dims[:dim], dims[dim] * dims[dim + 1], *dims[dim + 2 :])


def gathered_copies(x, axis, dim):
    tiles = copy_for_each(x, axis)
    return in_order(tiles, dim)


def passed_along(block, axis, distance):
    devices = range(lax.axis_size(axis))
    route = [(i - distance, i) for i in devices if i - distance in devices]
    return lax.ppermute(block, axis, route)


def slot_table(routes, experts, capacity):
    flattened = routes.reshape(-1)
    onehot = (flattened[:, None] == jnp.arange(experts, dtype=jnp.int32)[None, :]).astype(jnp.int32)
    earlier = jnp.cumsum(onehot, axis=0) - onehot
    return flattened * capacity + jnp.sum(earlier * onehot, axis=1)


def contract(left, right, left_dim, right_dim):
    return lax.dot_general(
        left, right, (((left_dim,), (right_dim,)), ((), ())), preferred_element_type=jnp.float32
    )


def on_device(
    moe_input,
    cotangent,
    route_ids,
    route_weights,
    expert_gate,
    expert_up,
    expert_down,
    out_proj,
    gate_b,
    gate_c,
    conv_in,
    taps,
):
    groups = lax.axis_size("sp")
    lanes = lax.axis_size("tp")
    token_count, model_width = moe_input.shape
    choices_count = route_ids.shape[1]
    experts = EXP_DEV * groups
    capacity = 2 * token_count * choices_count // experts
    assigned = token_count * choices_count
    slice_width = model_width // lanes
    column_start = lax.axis_index("tp") * slice_width
    slots = slot_table(route_ids, experts, capacity)
    owner = (
        jnp.full((experts * capacity,), assigned, jnp.int32)
        .at[slots]
        .set(jnp.arange(assigned, dtype=jnp.int32))
    )
    token_owner = jnp.where(owner < assigned, owner // choices_count, token_count)
    scaled = (
        (route_weights[:, :, None] * cotangent[:, None, :].astype(jnp.float32))
        .astype(jnp.bfloat16)
        .reshape(assigned, model_width)
    )

    def to_slots(values, positions):
        padded = jnp.concatenate([values, jnp.zeros((1, values.shape[1]), values.dtype)], axis=0)
        return padded[positions].reshape(experts, capacity, values.shape[1])

    slim_x = to_slots(
        lax.dynamic_slice_in_dim(moe_input, column_start, slice_width, 1), token_owner
    )
    slim_s = to_slots(lax.dynamic_slice_in_dim(scaled, column_start, slice_width, 1), owner)
    part_x, part_s = sent_together((slim_x, slim_s), "sp", 0, 0, 1)
    arrived_x, arrived_s = side_by_side((part_x, part_s), "tp", 2, 0)
    rows_x = arrived_x.reshape(-1, model_width)
    rows_s = arrived_s.reshape(-1, model_width)
    weight_gate = expert_gate[0]
    weight_up = expert_up[0]
    weight_down = expert_down[0]
    pre_gate = jnp.dot(rows_x, weight_gate, preferred_element_type=jnp.float32)
    pre_up = jnp.dot(rows_x, weight_up, preferred_element_type=jnp.float32)
    sigma = jax.nn.sigmoid(pre_gate)
    active = pre_gate * sigma
    hidden = (active * pre_up).astype(jnp.bfloat16)
    back = contract(rows_s, weight_down, 1, 1)
    grad_pre_gate = (back * pre_up * sigma * (1.0 + pre_gate * (1.0 - sigma))).astype(jnp.bfloat16)
    grad_pre_up = (back * active).astype(jnp.bfloat16)
    grad_down = contract(hidden, rows_s, 0, 0)
    grad_gate = contract(rows_x, grad_pre_gate, 0, 0)
    grad_up = contract(rows_x, grad_pre_up, 0, 0)
    partial_value = contract(grad_pre_gate, weight_gate, 1, 1) + contract(
        grad_pre_up, weight_up, 1, 1
    )
    summed = sum_at_owner(partial_value.astype(jnp.bfloat16), "tp", 1).astype(jnp.bfloat16)
    returned = lax.all_to_all(
        summed.reshape(groups, capacity, slice_width), "sp", split_axis=0, concat_axis=0, tiled=True
    )
    returned = returned.reshape(experts * capacity, slice_width)
    moe_rows = (
        returned[slots]
        .astype(jnp.float32)
        .reshape(token_count, choices_count, slice_width)
        .sum(axis=1)
    )
    own_cols = lax.dynamic_slice_in_dim(cotangent, column_start, slice_width, 1)
    grad_cols = (own_cols.astype(jnp.float32) + moe_rows).astype(jnp.bfloat16)
    stream_grad = gathered_copies(grad_cols, "tp", 1)
    mixed = gate_c.astype(jnp.float32) * conv_in.astype(jnp.float32)
    earlier_rows = passed_along(mixed[-2:], "sp", 1)
    extended = jnp.concatenate([earlier_rows, mixed], axis=0)
    conv = taps[2] * mixed + taps[1] * extended[1:-1] + taps[0] * extended[:-2]
    merged = (gate_b.astype(jnp.float32) * conv).astype(jnp.bfloat16)
    grad_merged = contract(stream_grad, out_proj, 1, 1)
    grad_gate_b = (grad_merged * conv).astype(jnp.bfloat16)
    grad_conv = grad_merged * gate_b.astype(jnp.float32)
    later_rows = passed_along(grad_conv[:2], "sp", -1)
    extended_grad = jnp.concatenate([grad_conv, later_rows], axis=0)
    grad_mixed = taps[2] * grad_conv + taps[1] * extended_grad[1:-1] + taps[0] * extended_grad[2:]
    grad_gate_c = (grad_mixed * conv_in.astype(jnp.float32)).astype(jnp.bfloat16)
    grad_conv_in = (grad_mixed * gate_c.astype(jnp.float32)).astype(jnp.bfloat16)
    grad_proj = sum_at_owner(contract(stream_grad, merged, 0, 0).astype(jnp.bfloat16), "sp", 0)
    return (
        grad_gate[None],
        grad_up[None],
        grad_down[None],
        grad_proj.T,
        grad_gate_b,
        grad_gate_c,
        grad_conv_in,
    )


def solution(mesh):
    placed = (
        P("sp", None),
        P("sp", None),
        P("sp", None),
        P("sp", None),
        P("sp", None, "tp"),
        P("sp", None, "tp"),
        P("sp", "tp", None),
        P("tp", None),
        P("sp", "tp"),
        P("sp", "tp"),
        P("sp", "tp"),
        P(None, "tp"),
    )
    return jax.shard_map(
        on_device,
        mesh=mesh,
        in_specs=placed,
        out_specs=(
            P("sp", None, "tp"),
            P("sp", None, "tp"),
            P("sp", "tp", None),
            P("tp", "sp"),
            P("sp", "tp"),
            P("sp", "tp"),
            P("sp", "tp"),
        ),
        check_vma=False,
    )
```

profile of v0, /device:TPU:1, one launch (start us, length us, event | category | flops | bytes accessed | tf_op | source)
XLA Modules:
  0.0 317.1 jit_solution(1026629322150247559)
XLA Ops:
  8.8 4.1 %mul.134 = f32[176,2,2048]{2,1,0:T(2,128)} broadcast(bf16[176,2048]{1,0:T(8,128)(2,1)} %param.13), dimensions={0,2} | broadcast | bytes 3604480 | tf_op jit(solution)/shard_map/mul | solution.py:103
  12.9 4.9 %mul.135 = f32[352,2048]{1,0:T(8,128)} reshape(f32[176,2,2048]{2,1,0:T(2,128)} %mul.134) | data formatting | bytes 5767168 | tf_op jit(solution)/shard_map/mul | solution.py:103
  19.9 2.9 scatter_custom_fusion
  22.8 1.0 fusion.16
  23.9 2.0 gather_fusion.1
  26.0 2.0 gather_fusion
  28.2 44.3 %all_to_all.25 = bf16[32,44,128]{2,1,0:T(8,128)(2,1)S(1)} all-to-all(bf16[32,44,128]{2,1,0:T(8,128)(2,1)S(1)} %pad_maximum_fusion), channel_id=1, replica_groups=mesh['sp'=32,'tp'=16] {'sp'}, dimensions={0} | all-to-all | bytes 720896 | tf_op jit(solution)/shard_map/all_to_all | solution.py:12
  73.4 72.4 %all-gather.2.cloned.1.call-done = bf16[64,22,2048]{2,1,0:T(8,128)(2,1)} async-done(((bf16[64,22,128]{2,1,0:T(8,128)(2,1)}), bf16[64,22,2048]{2,1,0:T(8,128)(2,1)}) %all-gather.2.cloned.1.call-update) | async-done | bytes 5767184 | tf_op jit(solution)/shard_map/all_gather | solution.py:22
  145.9 6.6 %fusion.43 = (bf16[32,22,2048]{2,1,0:T(8,128)(2,1)}, bf16[32,22,2048]{2,1,0:T(8,128)(2,1)}) fusion(bf16[64,22,2048]{2,1,0:T(8,128)(2,1)} %all-gather.2.cloned.1.call-done), kind=kLoop, calls=%fused_computation.95 | loop fusion | bytes 11534336 | tf_op jit(solution)/shard_map/split | solution.py:22
  152.5 4.5 %reshape.98 = bf16[704,2048]{1,0:T(8,128)(2,1)} reshape(bf16[32,22,2048]{2,1,0:T(8,128)(2,1)} %get-tuple-element.12) | data formatting | bytes 5767168 | tf_op jit(solution)/shard_map/reshape | solution.py:118
  157.0 2.9 fusion.8
  159.9 1.0 fusion.11
  160.9 4.5 %reshape.99 = bf16[704,2048]{1,0:T(8,128)(2,1)} reshape(bf16[32,22,2048]{2,1,0:T(8,128)(2,1)} %get-tuple-element.11) | data formatting | bytes 5767168 | tf_op jit(solution)/shard_map/reshape | solution.py:119
  165.4 2.8 multiply_convert_fusion.1
  170.8 40.3 %all_to_all.26 = bf16[16,704,128]{2,1,0:T(8,128)(2,1)} all-to-all(bf16[16,704,128]{2,1,0:T(8,128)(2,1)S(1)} %bitcast.78), channel_id=1, replica_groups=mesh['sp'=32,'tp'=16] {'tp'}, dimensions={0} | all-to-all | bytes 5767168 | tf_op jit(solution)/shard_map/all_to_all | solution.py:33
  211.1 2.2 reduce_sum.43
  214.2 15.5 %all-to-all-start.2 = ((bf16[32,22,128]{2,1,0:T(8,128)(2,1)}), bf16[32,22,128]{2,1,0:T(8,128)(2,1)S(1)}, u32[]{:S(2)}, u32[]{:S(2)}) async-start(bf16[32,22,128]{2,1,0:T(8,128)(2,1)} %reshape.101), calls=%async_computation.2 | async-start | bytes 393216 | tf_op jit(solution)/shard_map/all_to_all | solution.py:138
  229.7 18.8 %all-to-all-done.2 = bf16[32,22,128]{2,1,0:T(8,128)(2,1)S(1)} async-done(((bf16[32,22,128]{2,1,0:T(8,128)(2,1)}), bf16[32,22,128]{2,1,0:T(8,128)(2,1)S(1)}, u32[]{:S(2)}, u32[]{:S(2)}) %all-to-all-start.2) | async-done | bytes 180256 | tf_op jit(solution)/shard_map/all_to_all | solution.py:138
  248.5 1.4 gather_fusion.2
  251.0 1.0 broadcast_in_dim.36
  252.0 3.6 %all-to-all-start.3 = ((bf16[16,176,128]{2,1,0:T(8,128)(2,1)}), bf16[16,176,128]{2,1,0:T(8,128)(2,1)S(1)}, u32[]{:S(2)}, u32[]{:S(2)}) async-start(bf16[16,176,128]{2,1,0:T(8,128)(2,1)} %broadcast_in_dim.36), calls=%async_computation.3 | async-start | bytes 1441792 | tf_op jit(solution)/shard_map/all_to_all | solution.py:39
  255.7 3.3 %collective-permute-start = (f32[2,128]{1,0:T(2,128)S(1)}, f32[2,128]{1,0:T(2,128)S(1)}, u32[]{:S(2)}, u32[]{:S(2)}) collective-permute-start(f32[2,128]{1,0:T(2,128)S(1)} %slice.59), channel_id=1, source_target_pairs={{0,16},{16,32},{32,48},{48,64},{64,80},{80,96},{96,112},{112,128},... | collective-permute-start | bytes 3080 | tf_op jit(solution)/shard_map/ppermute | solution.py:56
  259.7 8.0 %all-to-all-done.3 = bf16[16,176,128]{2,1,0:T(8,128)(2,1)S(1)} async-done(((bf16[16,176,128]{2,1,0:T(8,128)(2,1)}), bf16[16,176,128]{2,1,0:T(8,128)(2,1)S(1)}, u32[]{:S(2)}, u32[]{:S(2)}) %all-to-all-start.3) | async-done | bytes 720928 | tf_op jit(solution)/shard_map/all_to_all | solution.py:39
  267.7 1.0 multiply_convert_fusion.4
  268.6 1.3 convolution_convert_fusion
  269.9 6.1 %all-to-all-start.4 = ((bf16[32,64,128]{2,1,0:T(8,128)(2,1)}), bf16[32,64,128]{2,1,0:T(8,128)(2,1)S(1)}, u32[]{:S(2)}, u32[]{:S(2)}) async-start(bf16[32,64,128]{2,1,0:T(8,128)(2,1)} %bitcast.13), calls=%async_computation.4 | async-start | bytes 1048576 | tf_op jit(solution)/shard_map/all_to_all | solution.py:33
  276.0 3.4 %convolution_bitcast_fusion.1 = f32[1,2048,64]{1,2,0:T(8,128)} fusion(bf16[704,64]{0,1:T(8,128)(2,1)S(1)} %get-tuple-element.14, bf16[704,2048]{1,0:T(8,128)(2,1)} %reshape.98), kind=kOutput, calls=%fused_computation.8 | convolution fusion | flops 184549376 | bytes 3497984 | tf_op jit(solution)/shard_map/dot_general | solution.py:67
  279.4 3.2 %convolution_bitcast_fusion.2 = f32[1,64,2048]{2,1,0:T(8,128)} fusion(bf16[704,2048]{1,0:T(8,128)(2,1)} %reshape.99, f32[704,64]{0,1:T(8,128)S(1)} %fusion.11, f32[704,64]{0,1:T(8,128)S(1)} %fusion.8), kind=kOutput, calls=%fused_computation.9 | convolution fusion | flops 184819712 | bytes 3768320 | tf_op jit(solution)/shard_map/dot_general | solution.py:67
  282.6 2.2 collective-permute-start.1
  284.9 1.4 convolution_bitcast_fusion
  286.3 13.1 %collective-permute-done.1 = f32[2,128]{1,0:T(2,128)S(1)} collective-permute-done((f32[2,128]{1,0:T(2,128)S(1)}, f32[2,128]{1,0:T(2,128)S(1)}, u32[]{:S(2)}, u32[]{:S(2)}) %collective-permute-start.1) | collective-permute-done | bytes 1056 | tf_op jit(solution)/shard_map/ppermute | solution.py:56
  300.7 8.8 %all-to-all-done.4 = bf16[32,64,128]{2,1,0:T(8,128)(2,1)S(1)} async-done(((bf16[32,64,128]{2,1,0:T(8,128)(2,1)}), bf16[32,64,128]{2,1,0:T(8,128)(2,1)S(1)}, u32[]{:S(2)}, u32[]{:S(2)}) %all-to-all-start.4) | async-done | bytes 524320 | tf_op jit(solution)/shard_map/all_to_all | solution.py:33
  (68 shorter events, 11.9 us)
Async XLA Ops:
  7.2 18.8 %copy-start = (bf16[176,2048]{1,0:T(8,128)(2,1)S(1)}, bf16[176,2048]{1,0:T(8,128)(2,1)}, u32[]{:S(2)}) copy-start(bf16[176,2048]{1,0:T(8,128)(2,1)} %param.12) | copy-start | bytes 2162692
  7.2 138.7 %all-gather.2.cloned.1.call-start = ((), (), s32[]{:S(2)}) async-start(), calls=%async_computation.5 | async-start | bytes 6684672 | tf_op jit(solution)/shard_map/all_gather | solution.py:22
  12.9 4.9 %copy-start.8 = (f32[176,2]{0,1:T(2,128)S(1)}, f32[176,2]{0,1:T(2,128)}, u32[]{:S(2)}) copy-start(f32[176,2]{0,1:T(2,128)} %param.15) | copy-start | bytes 4228
  152.5 4.5 %copy-start.3 = (bf16[1,2048,64]{1,2,0:T(8,128)(2,1)S(1)}, bf16[1,2048,64]{1,2,0:T(8,128)(2,1)}, u32[]{:S(2)}) copy-start(bf16[1,2048,64]{1,2,0:T(8,128)(2,1)} %param.16) | copy-start | bytes 786436
  157.0 2.9 copy-start.1
  157.0 2.9 copy-start.4
  160.9 4.5 %copy-start.11 = (bf16[1,64,2048]{2,1,0:T(8,128)(2,1)S(1)}, bf16[1,64,2048]{2,1,0:T(8,128)(2,1)}, u32[]{:S(2)}) copy-start(bf16[1,64,2048]{2,1,0:T(8,128)(2,1)} %param.18) | copy-start | bytes 786436
  213.4 42.2 %copy-start.5 = (bf16[176,128]{1,0:T(8,128)(2,1)S(1)}, bf16[176,128]{1,0:T(8,128)(2,1)}, u32[]{:S(2)}) copy-start(bf16[176,128]{1,0:T(8,128)(2,1)} %param.21) | copy-start | bytes 135172
  213.4 42.2 %copy-start.6 = (bf16[176,128]{1,0:T(8,128)(2,1)S(1)}, bf16[176,128]{1,0:T(8,128)(2,1)}, u32[]{:S(2)}) copy-start(bf16[176,128]{1,0:T(8,128)(2,1)} %param.22) | copy-start | bytes 135172
  213.4 45.6 %copy-start.9 = (f32[3,128]{1,0:T(4,128)S(1)}, f32[3,128]{1,0:T(4,128)}, u32[]{:S(2)}) copy-start(f32[3,128]{1,0:T(4,128)} %param.23) | copy-start | bytes 4612
  213.4 54.2 %copy-start.7 = (bf16[176,128]{1,0:T(8,128)(2,1)S(1)}, bf16[176,128]{1,0:T(8,128)(2,1)}, u32[]{:S(2)}) copy-start(bf16[176,128]{1,0:T(8,128)(2,1)} %param.20) | copy-start | bytes 135172
  213.4 54.2 %copy-start.10 = (bf16[128,2048]{1,0:T(8,128)(2,1)S(1)}, bf16[128,2048]{1,0:T(8,128)(2,1)}, u32[]{:S(2)}) copy-start(bf16[128,2048]{1,0:T(8,128)(2,1)} %param.19) | copy-start | bytes 1572868
  214.2 34.3 %all-to-all-start.2 = ((bf16[32,22,128]{2,1,0:T(8,128)(2,1)}), bf16[32,22,128]{2,1,0:T(8,128)(2,1)S(1)}, u32[]{:S(2)}, u32[]{:S(2)}) async-start(bf16[32,22,128]{2,1,0:T(8,128)(2,1)} %reshape.101), calls=%async_computation.2 | async-start | bytes 393216 | tf_op jit(solution)/shard_map/all_to_all | solution.py:138
  252.0 15.7 %all-to-all-start.3 = ((bf16[16,176,128]{2,1,0:T(8,128)(2,1)}), bf16[16,176,128]{2,1,0:T(8,128)(2,1)S(1)}, u32[]{:S(2)}, u32[]{:S(2)}) async-start(bf16[16,176,128]{2,1,0:T(8,128)(2,1)} %broadcast_in_dim.36), calls=%async_computation.3 | async-start | bytes 1441792 | tf_op jit(solution)/shard_map/all_to_all | solution.py:39
  255.7 4.0 %collective-permute-start = (f32[2,128]{1,0:T(2,128)S(1)}, f32[2,128]{1,0:T(2,128)S(1)}, u32[]{:S(2)}, u32[]{:S(2)}) collective-permute-start(f32[2,128]{1,0:T(2,128)S(1)} %slice.59), channel_id=1, source_target_pairs={{0,16},{16,32},{32,48},{48,64},{64,80},{80,96},{96,112},{112,128},... | collective-permute-start | bytes 3080 | tf_op jit(solution)/shard_map/ppermute | solution.py:56
  269.9 39.6 %all-to-all-start.4 = ((bf16[32,64,128]{2,1,0:T(8,128)(2,1)}), bf16[32,64,128]{2,1,0:T(8,128)(2,1)S(1)}, u32[]{:S(2)}, u32[]{:S(2)}) async-start(bf16[32,64,128]{2,1,0:T(8,128)(2,1)} %bitcast.13), calls=%async_computation.4 | async-start | bytes 1048576 | tf_op jit(solution)/shard_map/all_to_all | solution.py:33
  276.0 8.9 %copy-start.2 = (bf16[704,2048]{1,0:T(8,128)(2,1)S(1)}, bf16[704,2048]{1,0:T(8,128)(2,1)}, u32[]{:S(2)}) copy-start(bf16[704,2048]{1,0:T(8,128)(2,1)} %reshape.98) | copy-start | bytes 8650756
  282.6 16.8 %collective-permute-start.1 = (f32[2,128]{1,0:T(2,128)S(1)}, f32[2,128]{1,0:T(2,128)S(1)}, u32[]{:S(2)}, u32[]{:S(2)}) collective-permute-start(f32[2,128]{1,0:T(2,128)S(1)} %slice.62), channel_id=1, source_target_pairs={{16,0},{32,16},{48,32},{64,48},{80,64},{96,80},{112,96},{128,112},... | collective-permute-start | bytes 3080 | tf_op jit(solution)/shard_map/ppermute | solution.py:56
Sparse Core Ops, SparseCore 0:
  73.5 72.2 all-gather.1
where the time goes:
time: 318 us; the launch traced here: 317 us
  waiting for transfers between devices  122 us (38%)
  blocking collectives  84.6 us (27%)
  local copies, waits for them, and re-layouts  37.5 us (12%)
  starting transfers between devices  30.7 us (10%)
  matrix products  18.8 us (6%)
  between operations  14.5 us (5%)
  other arithmetic  9.08 us (3%)
    all_gather x1, waiting for transfers between devices, side_by_side(): lax.all_gather(both, axis, axis=dim, tiled=True)  72.4 us
    all_to_all x1, blocking collectives, sent_together(): lax.all_to_all(both, axis, split_axis=split_dim, concat_axis=concat_dim,...  44.3 us
    all_to_all x1, blocking collectives, sum_at_owner(): tiles = lax.all_to_all(split_up(x, dim, devices), axis, 0, 0, tiled=True)  40.3 us
    all_to_all x1, waiting for transfers between devices, on_device(): lax.all_to_all(summed.reshape(groups, capacity, slice_width), 'sp', split...  18.8 us
    all_to_all x1, starting transfers between devices, on_device(): lax.all_to_all(summed.reshape(groups, capacity, slice_width), 'sp', split...  15.5 us
    dot_general x8, matrix products, contract(): lax.dot_general(left, right, (((left_dim,), (right_dim,)), ((), ())), pre...  14.9 us
    ppermute x2, waiting for transfers between devices, passed_along(): return lax.ppermute(block, axis, route)  13.8 us
    mul x3, local copies, waits for them, and re-layouts, on_device(): route_weights[:, :, None] * cotangent[:, None, :].astype(jnp.float32)  9.22 us
  transfers between devices with their start and end apart: 6, of which 6 were waited for; matrix products, arithmetic and copies ran while one was open for 3% of the time, Pallas kernels for 0%

commit v1 on v0

v1 whole, which is shorter than its diff:
```python
import functools

import jax
import jax.numpy as jnp
from jax import lax
from jax.experimental import pallas as pl
from jax.experimental.pallas import tpu as pltpu
from jax.sharding import PartitionSpec as P

MESH = pl.DeviceIdType.MESH
BF = jnp.bfloat16
F32 = jnp.float32
NX = 4
NY = 4
W = 128


def dot(a, b, ca, cb):
    return lax.dot_general(a, b, (((ca,), (cb,)), ((), ())), preferred_element_type=F32)


def kernel(
    ns, cp,
    ids_ref, wts_ref, x_hbm, c_hbm, wg_hbm, wu_hbm, wd_hbm, op_hbm, gb_ref, gc_ref, ci_ref, taps_ref,
    gg_out, gu_out, gd_out, gp_out, ggb_out, ggc_out, gci_out,
    xcol, ccol, opv, disp, gx, wx, rows, preb, rs1, rs2, act, slotp, xr1, xr2, ret, retr, pt, st,
    gs, gr, mhs, mh, ghs, gh, gpo, gpp, pr, gq, fr,
    loc_sem, bsem_w, wsem_s, wsem_r, d_s, d_r, gx_s, gx_r, gxf_s, gxf_r, y_s, y_r, a_s, a_r, af_s, af_r,
    xs_s, xs_r, r_s, r_r, st_s, st_r, gw_s, gw_r, h_s, h_r, p_s, p_r, f_s, f_r,
):
    me = lax.axis_index("sp")
    tp = lax.axis_index("tp")
    ym = lax.div(tp, NX)
    xm = lax.rem(tp, NX)
    core = lax.rem(me, 2)
    zm = lax.div(me, 2)
    nz = ns // 2
    t = ids_ref.shape[1]
    n_rows = ns * cp
    nq = ns // 4
    qr = nq * cp
    qh = qr // 2
    half = n_rows // 2

    def xdev(d):
        return ym * NX + lax.rem(xm + d, NX)

    def ydev(d):
        return lax.rem(ym + d, NY) * NX + xm

    def rc(src, dst, ss, rs, **where):
        return pltpu.make_async_remote_copy(
            src_ref=src, dst_ref=dst, send_sem=ss, recv_sem=rs, device_id=where, device_id_type=MESH
        )

    barrier = pltpu.get_barrier_semaphore()

    @pl.loop(1, ns)
    def _(d):
        pl.semaphore_signal(barrier, inc=1, device_id={"sp": lax.rem(me + d, ns)}, device_id_type=MESH)

    @pl.loop(1, NX * NY)
    def _(d):
        pl.semaphore_signal(barrier, inc=1, device_id={"tp": lax.rem(tp + d, NX * NY)}, device_id_type=MESH)

    cols = pl.ds(pl.multiple_of(tp * W, W), W)
    yb = 4 * W
    load_x = pltpu.make_async_copy(x_hbm.at[:, cols], xcol, loc_sem.at[0])
    load_c = pltpu.make_async_copy(c_hbm.at[:, cols], ccol, loc_sem.at[1])
    load_o = pltpu.make_async_copy(op_hbm, opv, loc_sem.at[2])
    mats = (wg_hbm, wu_hbm, wd_hbm)
    ycols = pl.ds(pl.multiple_of(ym * yb, yb), yb)
    load_w = [pltpu.make_async_copy(mats[m].at[:, ycols], wx.at[ym, m], bsem_w.at[m]) for m in range(3)]
    load_x.start()
    load_c.start()
    for m in range(3):
        load_w[m].start()
    load_o.start()

    id0 = ids_ref[0:1, :]
    id1 = ids_ref[1:2, :]
    eio = lax.broadcasted_iota(jnp.int32, (ns, t), 0)
    oh0 = (eio == id0).astype(F32)
    oh1 = (eio == id1).astype(F32)
    before = (lax.broadcasted_iota(jnp.int32, (t, t), 0) < lax.broadcasted_iota(jnp.int32, (t, t), 1)).astype(F32).astype(BF)
    cum = dot((oh0 + oh1).astype(BF), before, 1, 0)
    slot0 = id0 * cp + jnp.sum(oh0 * cum, axis=0, keepdims=True).astype(jnp.int32)
    slot1 = id1 * cp + jnp.sum(oh1 * cum, axis=0, keepdims=True).astype(jnp.int32)
    rio = lax.broadcasted_iota(jnp.int32, (n_rows, t), 0)
    p0 = rio == slot0
    p1 = rio == slot1
    pmat = jnp.where(p0 | p1, 1.0, 0.0)
    wslot = jnp.sum(jnp.where(p0, wts_ref[0:1, :], jnp.where(p1, wts_ref[1:2, :], 0.0)), axis=1, keepdims=True)
    pb = pmat.astype(BF)
    load_x.wait()
    load_c.wait()
    picked = dot(pb, jnp.concatenate([xcol[...], ccol[...]], axis=1), 1, 0)
    disp[:, 0] = picked[:, :W].reshape(ns, cp, W).astype(BF)
    disp[:, 1] = (wslot * picked[:, W:]).reshape(ns, cp, W).astype(BF)

    mixed = gc_ref[...].astype(F32) * ci_ref[...].astype(F32)
    mhs[...] = mixed[t - 8 :, :]

    pl.semaphore_wait(barrier, ns - 1 + NX * NY - 1)

    def dispatch(d):
        i = lax.rem(me + d, ns)
        return rc(disp.at[i], gx.at[xm, me], d_s.at[i], d_r.at[me], sp=i)

    def arrival(i):
        return rc(disp.at[i], gx.at[xm, i], d_s.at[i], d_r.at[i], sp=i)

    @pl.loop(1, ns)
    def _(d):
        dispatch(d).start()

    halo_m = rc(mhs, mh, h_s.at[0], h_r.at[0], sp=lax.rem(me + 1, ns))
    halo_m.start()

    def wcopy(d, m, dst):
        block = pl.ds(pl.multiple_of(lax.rem(ym + d, NY) * yb, yb), yb)
        return rc(mats[m].at[:, block], wx.at[dst, m], wsem_s.at[d - 1, m], wsem_r.at[d - 1, m], tp=ydev(d))

    def wsend(d, m):
        return wcopy(d, m, ym)

    def wrecv(d, m):
        return wcopy(d, m, lax.rem(ym - d + NY, NY))

    for d in (1, 3, 2):
        for m in range(3):
            wsend(d, m).start()

    gx[xm, me] = disp[me]

    pt[...] = pmat.T.astype(BF)

    def gsend(q, s):
        part = pl.ds(q * nq, nq)
        d = 1 if s == 0 else NX - 1
        return rc(gx.at[xm, part], gx.at[xm, part], gx_s.at[s, q], gx_r.at[s, q], tp=xdev(d))

    def grecv(q, s):
        part = pl.ds(q * nq, nq)
        d = NX - 1 if s == 0 else 1
        src = lax.rem(xm + d, NX)
        return rc(gx.at[xm, part], gx.at[src, part], gx_s.at[s, q], gx_r.at[s, q], tp=xdev(d))

    def gforward(q):
        part = pl.ds(q * nq, nq)
        s = 0 if q < 2 else 1
        src = lax.rem(xm + (NX - 1 if s == 0 else 1), NX)
        d = 1 if s == 0 else NX - 1
        return rc(gx.at[src, part], gx.at[src, part], gxf_s.at[q], gxf_r.at[q], tp=xdev(d))

    def gfar(q):
        part = pl.ds(q * nq, nq)
        far = lax.rem(xm + 2, NX)
        return rc(gx.at[far, part], gx.at[far, part], gxf_s.at[q], gxf_r.at[q], tp=xdev(2))

    for q in range(4):
        @pl.loop(0, nq)
        def _(k, q=q):
            i = q * nq + k

            @pl.when(i != me)
            def _():
                arrival(i).wait_recv()

        gsend(q, 0).start()
        gsend(q, 1).start()

    for q in range(4):
        if q < 2:
            grecv(q, 0).wait_recv()
            gforward(q).start()
            grecv(q, 1).wait_recv()
        else:
            grecv(q, 1).wait_recv()
            gforward(q).start()
            grecv(q, 0).wait_recv()

    for m in range(3):
        load_w[m].wait()
        for d in (1, 2, 3):
            wrecv(d, m).wait_recv()

    for q in range(4):
        gfar(q).wait_recv()
    w3 = [jnp.concatenate([wx[yy, m] for yy in range(NY)], axis=0) for m in range(3)]

    @pl.loop(0, 4)
    def _(q):
        for s in range(2):
            blocks = [gx[xx, pl.ds(q * nq, nq), s].astype(F32).reshape(qr, W) for xx in range(NX)]
            rows[s, q] = jnp.concatenate(blocks, axis=1).astype(BF)
        for m in range(3):
            preb[q, :, m * 2 * W : (m + 1) * 2 * W] = dot(rows[1 if m == 2 else 0, q], w3[m], 1, 1).astype(BF)

    low, high = pl.ds(0, qh), pl.ds(qh, qh)
    up, down, far = lax.rem(ym + 1, NY), lax.rem(ym + 3, NY), lax.rem(ym + 2, NY)
    y_far_up = rc(preb.at[far, low], rs1.at[0], y_s.at[0], y_r.at[0], tp=ydev(1))
    y_far_down = rc(preb.at[far, high], rs1.at[1], y_s.at[1], y_r.at[1], tp=ydev(3))
    y_up_b = rc(preb.at[up, high], rs2.at[0, high], y_s.at[2], y_r.at[2], tp=ydev(1))
    y_down_a = rc(preb.at[down, low], rs2.at[1, low], y_s.at[3], y_r.at[3], tp=ydev(3))
    y_up_a = rc(preb.at[up, low], rs2.at[0, low], y_s.at[4], y_r.at[4], tp=ydev(1))
    y_down_b = rc(preb.at[down, high], rs2.at[1, high], y_s.at[5], y_r.at[5], tp=ydev(3))
    y_far_up.start()
    y_far_down.start()
    y_up_b.start()
    y_down_a.start()
    y_far_up.wait_recv()
    preb[up, low] = (preb[up, low].astype(F32) + rs1[0].astype(F32)).astype(BF)
    y_up_a.start()
    y_far_down.wait_recv()
    preb[down, high] = (preb[down, high].astype(F32) + rs1[1].astype(F32)).astype(BF)
    y_down_b.start()
    y_up_b.wait_recv()
    y_down_a.wait_recv()
    y_up_a.wait_recv()
    y_down_b.wait_recv()
    u = 2 * W

    def total(m):
        c = slice(m * u, (m + 1) * u)
        return preb[ym, :, c].astype(F32) + rs2[0, :, c].astype(F32) + rs2[1, :, c].astype(F32)

    pre_gate = total(0)
    pre_up = total(1)
    back = total(2)
    sigma = jax.nn.sigmoid(pre_gate)
    active = pre_gate * sigma
    act[ym, :, 0:u] = (back * pre_up * sigma * (1.0 + pre_gate * (1.0 - sigma))).astype(BF)
    act[ym, :, u : 2 * u] = (back * active).astype(BF)
    act[ym, :, 2 * u :] = (active * pre_up).astype(BF)

    a_up = rc(act.at[ym], act.at[ym], a_s.at[0], a_r.at[0], tp=ydev(1))
    a_down = rc(act.at[ym], act.at[ym], a_s.at[1], a_r.at[1], tp=ydev(3))
    a_up.start()
    a_down.start()
    rc(act.at[ym], act.at[down], a_s.at[0], a_r.at[0], tp=ydev(3)).wait_recv()
    af_up = rc(act.at[down, low], act.at[down, low], af_s.at[0], af_r.at[0], tp=ydev(1))
    af_up.start()
    rc(act.at[ym], act.at[up], a_s.at[1], a_r.at[1], tp=ydev(1)).wait_recv()
    af_down = rc(act.at[up, high], act.at[up, high], af_s.at[1], af_r.at[1], tp=ydev(3))
    af_down.start()
    rc(act.at[far, low], act.at[far, low], af_s.at[0], af_r.at[0], tp=ydev(2)).wait_recv()
    rc(act.at[far, high], act.at[far, high], af_s.at[1], af_r.at[1], tp=ydev(2)).wait_recv()

    @pl.loop(0, 4)
    def _(q):
        part = dot(act[q, :, 0:u], w3[0], 1, 0) + dot(act[q, :, u : 2 * u], w3[1], 1, 0)
        for xx in range(NX):
            slotp[xx, pl.ds(pl.multiple_of(q * qr, qr), qr), :] = part[:, xx * W : (xx + 1) * W].astype(BF)

    lo, hi = pl.ds(0, half), pl.ds(half, half)
    xr, xl, xf = lax.rem(xm + 1, NX), lax.rem(xm + 3, NX), lax.rem(xm + 2, NX)
    x_far_r = rc(slotp.at[xf, lo], xr1.at[0], xs_s.at[0], xs_r.at[0], tp=xdev(1))
    x_far_l = rc(slotp.at[xf, hi], xr1.at[1], xs_s.at[1], xs_r.at[1], tp=xdev(3))
    x_r_b = rc(slotp.at[xr, hi], xr2.at[0, hi], xs_s.at[2], xs_r.at[2], tp=xdev(1))
    x_l_a = rc(slotp.at[xl, lo], xr2.at[1, lo], xs_s.at[3], xs_r.at[3], tp=xdev(3))
    x_r_a = rc(slotp.at[xr, lo], xr2.at[0, lo], xs_s.at[4], xs_r.at[4], tp=xdev(1))
    x_l_b = rc(slotp.at[xl, hi], xr2.at[1, hi], xs_s.at[5], xs_r.at[5], tp=xdev(3))
    x_far_r.start()
    x_far_l.start()
    x_r_b.start()
    x_l_a.start()
    x_far_r.wait_recv()
    slotp[xr, lo] = (slotp[xr, lo].astype(F32) + xr1[0].astype(F32)).astype(BF)
    x_r_a.start()
    x_far_l.wait_recv()
    slotp[xl, hi] = (slotp[xl, hi].astype(F32) + xr1[1].astype(F32)).astype(BF)
    x_l_b.start()

    for m in range(3):
        left = act[:, :, m * u : (m + 1) * u].reshape(n_rows, u)
        right = rows[1 if m == 2 else 0].reshape(n_rows, yb)
        gs[:, m] = dot(left, right, 0, 0).reshape(NY, 64, yb).astype(BF)

    def gwsend(d):
        return rc(gs.at[lax.rem(ym + d, NY)], gr.at[ym], gw_s.at[d - 1], gw_r.at[d - 1], tp=ydev(d))

    def gwrecv(d):
        return rc(gs.at[ym], gr.at[lax.rem(ym - d + NY, NY)], gw_s.at[d - 1], gw_r.at[d - 1], tp=ydev(d))

    x_r_b.wait_recv()
    x_l_a.wait_recv()
    x_r_a.wait_recv()
    x_l_b.wait_recv()
    slot = slotp[xm].astype(F32) + xr2[0].astype(F32) + xr2[1].astype(F32)
    ret[...] = slot.reshape(ns, cp, W).astype(BF)

    @pl.loop(1, ns)
    def _(d):
        i = lax.rem(me + d, ns)
        rc(ret.at[i], retr.at[me], r_s.at[i], r_r.at[me], sp=i).start()

    for d in (1, 3, 2):
        gwsend(d).start()
    retr[me] = ret[me]
    gr[ym] = gs[ym]

    halo_m.wait_recv()
    prev = jnp.where(me == 0, 0.0, mh[...])
    ext = jnp.concatenate([prev, mixed], axis=0)
    tap = taps_ref[...]
    conv = tap[2:3] * mixed + tap[1:2] * ext[7 : 7 + t] + tap[0:1] * ext[6 : 6 + t]
    merged = (gb_ref[...].astype(F32) * conv).astype(BF)

    @pl.loop(1, ns)
    def _(d):
        i = lax.rem(me + d, ns)
        rc(ret.at[i], retr.at[i], r_s.at[i], r_r.at[i], sp=i).wait_recv()

    back_rows = retr[...].astype(F32).reshape(n_rows, W).astype(BF)
    grad_cols = ccol[...].astype(F32) + dot(pt[...], back_rows, 1, 0)
    st[tp] = grad_cols.astype(BF)

    def stsend(d):
        return rc(st.at[tp], st.at[tp], st_s.at[d - 1], st_r.at[d - 1], tp=lax.rem(tp + d, NX * NY))

    def strecv(d):
        src = lax.rem(tp - d + NX * NY, NX * NY)
        return rc(st.at[tp], st.at[src], st_s.at[d - 1], st_r.at[d - 1], tp=src)

    @pl.loop(1, NX * NY)
    def _(d):
        stsend(d).start()

    for d in (1, 2, 3):
        gwrecv(d).wait_recv()
    for m, out in enumerate((gg_out, gu_out, gd_out)):
        for yy in range(NY):
            out[:, yy * yb : (yy + 1) * yb] = gr[yy, m].astype(F32)
    load_o.wait()

    @pl.loop(1, NX * NY)
    def _(d):
        strecv(d).wait_recv()

    stream = jnp.concatenate([st[j] for j in range(NX * NY)], axis=1)
    grad_merged = dot(stream, opv[...], 1, 1)
    grad_conv = grad_merged * gb_ref[...].astype(F32)
    ghs[...] = grad_conv[0:8, :]
    halo_g = rc(ghs, gh, h_s.at[1], h_r.at[1], sp=lax.rem(me + ns - 1, ns))
    halo_g.start()

    proj = dot(stream, merged, 0, 0).reshape(NX * NY, 2, 64, W)
    proj0 = proj[:, 0]
    proj1 = proj[:, 1]
    gpo[...] = jnp.where(core == 0, proj0, proj1)
    gpp[...] = jnp.where(core == 0, proj1, proj0).astype(BF)
    pair = rc(gpp, pr, p_s.at[0], p_r.at[0], sp=zm * 2 + 1 - core)
    pair.start()
    ggb_out[...] = (grad_merged * conv).astype(BF)
    pair.wait_recv()
    gpo[...] = gpo[...] + pr[...].astype(F32)
    gq[...] = gpo[...].astype(BF)

    @pl.loop(1, nz)
    def _(d):
        z = lax.rem(zm + d, nz)
        rc(gq.at[z], fr.at[zm], f_s.at[z], f_r.at[zm], sp=z * 2 + core).start()

    halo_g.wait_recv()
    following = jnp.where(me == ns - 1, 0.0, gh[...])
    extg = jnp.concatenate([grad_conv, following], axis=0)
    grad_mixed = tap[2:3] * grad_conv + tap[1:2] * extg[1 : 1 + t] + tap[0:1] * extg[2 : 2 + t]
    ggc_out[...] = (grad_mixed * ci_ref[...].astype(F32)).astype(BF)
    gci_out[...] = (grad_mixed * gc_ref[...].astype(F32)).astype(BF)

    @pl.loop(1, ns)
    def _(d):
        dispatch(d).wait_send()
        i = lax.rem(me + d, ns)
        rc(ret.at[i], retr.at[me], r_s.at[i], r_r.at[me], sp=i).wait_send()

    halo_m.wait_send()
    halo_g.wait_send()
    for d in (1, 2, 3):
        for m in range(3):
            wsend(d, m).wait_send()
        gwsend(d).wait_send()
    for q in range(4):
        gsend(q, 0).wait_send()
        gsend(q, 1).wait_send()
        gforward(q).wait_send()
    for c in (y_far_up, y_far_down, y_up_b, y_down_a, y_up_a, y_down_b, a_up, a_down, af_up, af_down):
        c.wait_send()
    for c in (x_far_r, x_far_l, x_r_b, x_l_a, x_r_a, x_l_b, pair):
        c.wait_send()

    @pl.loop(1, NX * NY)
    def _(d):
        stsend(d).wait_send()

    @pl.loop(1, nz)
    def _(d):
        z = lax.rem(zm + d, nz)
        rc(gq.at[z], fr.at[z], f_s.at[z], f_r.at[z], sp=z * 2 + core).wait()

    fr[zm] = gq[zm]
    gp_out[...] = jnp.sum(fr[...].astype(F32), axis=0)


def on_device(
    moe_input, cotangent, route_ids, route_weights, expert_gate, expert_up, expert_down,
    out_proj, gate_b, gate_c, conv_in, taps,
):
    ns = lax.axis_size("sp")
    t, model = moe_input.shape
    cap = 2 * t * route_ids.shape[1] // ns
    cp = -(-cap // 8) * 8
    n_rows = ns * cp
    qr = n_rows // 4
    yb = model // NY
    tpn = NX * NY
    units = expert_gate.shape[2]
    sds = jax.ShapeDtypeStruct
    vmem = pl.BlockSpec(memory_space=pltpu.VMEM)
    anym = pl.BlockSpec(memory_space=pl.ANY)
    dma = pltpu.SemaphoreType.DMA
    V = pltpu.VMEM
    scratch = [
        V((t, W), BF), V((t, W), BF), V((W, model), BF), V((ns, 2, cp, W), BF), V((NX, ns, 2, cp, W), BF),
        V((NY, 3, units, yb), BF), V((2, 4, qr, yb), BF), V((4, qr, 6 * W), BF), V((2, qr // 2, 6 * W), BF),
        V((2, qr, 6 * W), BF), V((4, qr, 6 * W), BF), V((NX, n_rows, W), BF), V((2, n_rows // 2, W), BF),
        V((2, n_rows, W), BF), V((ns, cp, W), BF), V((ns, cp, W), BF), V((t, n_rows), BF), V((tpn, t, W), BF),
        V((NY, 3, units, yb), BF), V((NY, 3, units, yb), BF), V((8, W), F32), V((8, W), F32), V((8, W), F32), V((8, W), F32),
        V((tpn, 64, W), F32), V((tpn, 64, W), BF), V((tpn, 64, W), BF), V((tpn, 64, W), BF), V((tpn, 64, W), BF),
        dma((3,)), dma((3,)), dma((3, 3)), dma((3, 3)), dma((ns,)), dma((ns,)), dma((2, 4)), dma((2, 4)), dma((4,)), dma((4,)),
        dma((6,)), dma((6,)), dma((2,)), dma((2,)), dma((2,)), dma((2,)),
        dma((6,)), dma((6,)), dma((ns,)), dma((ns,)), dma((tpn - 1,)), dma((tpn - 1,)), dma((3,)), dma((3,)), dma((2,)), dma((2,)),
        dma((1,)), dma((1,)), dma((ns // 2,)), dma((ns // 2,)),
    ]
    outs = pl.pallas_call(
        functools.partial(kernel, ns, cp),
        out_shape=(
            sds((units, model), F32), sds((units, model), F32), sds((units, model), F32), sds((64, W), F32),
            sds((t, W), BF), sds((t, W), BF), sds((t, W), BF),
        ),
        in_specs=[vmem, vmem] + [anym] * 6 + [vmem] * 4,
        out_specs=[vmem] * 7,
        scratch_shapes=scratch,
        compiler_params=pltpu.CompilerParams(collective_id=0, has_side_effects=True, vmem_limit_bytes=56 * 2**20),
    )(
        route_ids.T, route_weights.T, moe_input, cotangent, expert_gate[0].T, expert_up[0].T, expert_down[0],
        out_proj, gate_b, gate_c, conv_in, taps,
    )
    gg, gu, gd, gp, ggb, ggc, gci = outs
    return gg.T[None], gu.T[None], gd[None], gp.T, ggb, ggc, gci


def solution(mesh):
    row, cols = P("sp", None), P("sp", "tp")
    return jax.shard_map(
        on_device,
        mesh=mesh,
        in_specs=(
            row, row, row, row, P("sp", None, "tp"), P("sp", None, "tp"), P("sp", "tp", None), P("tp", None),
            cols, cols, cols, P(None, "tp"),
        ),
        out_specs=(
            P("sp", None, "tp"), P("sp", None, "tp"), P("sp", "tp", None), P("tp", "sp"), cols, cols, cols,
        ),
        check_vma=False,
    )
```

time: 318 us -> 138 us (0.43)
  Pallas kernels: 0 us -> 130 us
  waiting for transfers between devices: 122 us -> 0 us
  blocking collectives: 84.6 us -> 0 us
  starting transfers between devices: 30.7 us -> 0 us
  local copies, waits for them, and re-layouts: 37.5 us -> 6.99 us
  matrix products: 18.8 us -> 0 us
  between operations: 14.5 us -> 0.66 us
  other arithmetic: 9.08 us -> 0 us
    pallas_call x0 -> x1, Pallas kernels: none -> 130 us  [on_device(): pl.pallas_call(functools.partial(kernel, ns, cp), out_shape=(sds((units,...]
    all_to_all x2 -> x0, blocking collectives: 84.6 us -> none  [the longest x1 44.3 us: sent_together(): lax.all_to_all(both, axis, split_axis=split_dim, concat_axis=concat_dim,...]
    all_gather x1 -> x0, waiting for transfers between devices: 72.4 us -> none  [side_by_side(): lax.all_gather(both, axis, axis=dim, tiled=True)]
    all_to_all x3 -> x0, waiting for transfers between devices: 35.6 us -> none  [the longest x1 18.8 us: on_device(): lax.all_to_all(summed.reshape(groups, capacity, slice_width), 'sp', split...]
    all_to_all x3 -> x0, starting transfers between devices: 25.2 us -> none  [the longest x1 15.5 us: on_device(): lax.all_to_all(summed.reshape(groups, capacity, slice_width), 'sp', split...]
    dot_general x10 -> x0, matrix products: 18.8 us -> none  [the longest x8 14.9 us: contract(): lax.dot_general(left, right, (((left_dim,), (right_dim,)), ((), ())), pre...]
    ppermute x2 -> x0, waiting for transfers between devices: 13.8 us -> none  [passed_along(): return lax.ppermute(block, axis, route)]
    reshape x7 -> x0, local copies, waits for them, and re-layouts: 10.6 us -> none  [the longest x1 4.49 us: on_device(): rows_s = arrived_s.reshape(-1, model_width)]
  transfers between devices with their start and end apart: 6 -> 0, of which waited for: 6 -> 0; matrix products, arithmetic and copies ran while one was open for 3% -> 0% of each run, Pallas kernels for 0% -> 0%
where the time goes in v1:
time: 138 us; the launch traced here: 137 us
  Pallas kernels  130 us (94%)
  local copies, waits for them, and re-layouts  6.99 us (5%)
    pallas_call x1, Pallas kernels, on_device(): pl.pallas_call(functools.partial(kernel, ns, cp), out_shape=(sds((units,...  130 us
    unnamed x19, local copies, waits for them, and re-layouts  6.99 us

profile of v1, /device:TPU:1, one launch (start us, length us, event | category | flops | bytes accessed | tf_op | source)
XLA Modules:
  0.0 137.3 jit_solution(4698423709148225050)
XLA Ops:
  0.6 129.6 %shard_map.171 = (f32[64,2048]{1,0:T(8,128)}, f32[64,2048]{1,0:T(8,128)}, f32[64,2048]{1,0:T(8,128)}, f32[64,128]{1,0:T(8,128)}, bf16[176,128]{1,0:T(8,128)(2,1)...) custom-call(s32[2,176]{1,0:T(2,128)} %bitcast.24, f32[2,176]{1,0:T(2,128)} %bitcast.25, bf16[176,2048]{1,0:T(8,128)(2,1)} %x_hbm.1, ...), custom_call_target="tpu_custom_call" | custom-call | tf_op jit(solution)/shard_map/pallas_call | solution.py:436
  130.3 0.0 copy-start.1
  130.3 1.9 %copy.26 = f32[1,2048,64]{1,2,0:T(8,128)} copy(f32[1,2048,64]{1,2,0:T(8,128)} %bitcast.19) | data formatting | bytes 1048576
  132.2 0.0 copy-done.1
  132.2 0.0 copy-start
  132.2 0.8 copy.27
  133.0 0.4 copy-done
  133.4 0.0 copy-start.5
  133.4 0.8 copy.28
  134.2 0.0 copy-done.5
  134.2 0.0 copy-start.4
  134.2 0.6 copy.29
  134.9 0.2 copy-done.4
  135.0 0.0 copy-start.3
  135.0 0.6 copy.30
  135.7 0.2 copy-done.3
  135.8 0.0 copy-start.2
  135.8 0.6 copy.31
  136.5 0.2 copy-done.2
  136.6 0.6 copy.32
Async XLA Ops:
  130.3 1.9 %copy-start.1 = (f32[64,2048]{1,0:T(8,128)S(1)}, f32[64,2048]{1,0:T(8,128)}, u32[]{:S(2)}) copy-start(f32[64,2048]{1,0:T(8,128)} %get-tuple-element.15) | copy-start | bytes 1572868
  132.2 1.2 copy-start
  133.4 0.8 copy-start.5
  134.2 0.8 copy-start.4
  135.0 0.8 copy-start.3
  135.8 0.8 copy-start.2

commit v2 on v1

v2 whole, which is shorter than its diff:
```python
import functools

import jax
import jax.numpy as jnp
from jax import lax
from jax.experimental import pallas as pl
from jax.experimental.pallas import tpu as pltpu
from jax.sharding import PartitionSpec as P

MESH = pl.DeviceIdType.MESH
BF = jnp.bfloat16
F32 = jnp.float32
NX = 4
NY = 4
W = 128


def dot(a, b, ca, cb):
    return lax.dot_general(a, b, (((ca,), (cb,)), ((), ())), preferred_element_type=F32)


CHUNKS = (16, 8, 8)
STARTS = tuple(sum(CHUNKS[:k]) for k in range(len(CHUNKS)))
NC = len(CHUNKS)
LAG = 1
ORDER = (0, 1, 3, 2)


def kernel(
    ns, cp,
    ids_hbm, wts_hbm, x_hbm, c_hbm, wg_hbm, wu_hbm, wd_hbm, op_hbm, gb_hbm, gc_hbm, ci_hbm, taps_hbm,
    gg_out, gu_out, gd_out, gp_out, ggb_out, ggc_out, gci_out,
    ids_ref, wts_ref, gb_ref, gc_ref, ci_ref, taps_ref,
    xcol, ccol, opv, disp, gx, wx, rows, preb, rs1, rs2, act, slotp, xr1, xr2, ret, retr, pt, st,
    gs, gr, mhs, mh, ghs, gh, gpo, gpp, pr, gq, fr,
    loc_sem, bsem_w, wsem_s, wsem_r, d_s, d_r, gx_s, gx_r, gxf_s, gxf_r, y_s, y_r, a_s, a_r, af_s, af_r,
    xs_s, xs_r, r_s, r_r, st_s, st_r, gw_s, gw_r, h_s, h_r, p_s, p_r, f_s, f_r,
):
    me = lax.axis_index("sp")
    tp = lax.axis_index("tp")
    ym = lax.div(tp, NX)
    xm = lax.rem(tp, NX)
    core = lax.rem(me, 2)
    zm = lax.div(me, 2)
    nz = ns // 2
    t = ids_ref.shape[1]
    n_rows = ns * cp
    u = 2 * W
    yb = 4 * W

    def xdev(d):
        return ym * NX + lax.rem(xm + d, NX)

    def ydev(d):
        return lax.rem(ym + d, NY) * NX + xm

    def rc(src, dst, ss, rs, **where):
        return pltpu.make_async_remote_copy(
            src_ref=src, dst_ref=dst, send_sem=ss, recv_sem=rs, device_id=where, device_id_type=MESH
        )

    def offset(k):
        return lax.div(k + 1, 2) * (2 * lax.rem(k, 2) - 1)

    sends = []

    def go(copy):
        copy.start()
        sends.append(copy)

    barrier = pltpu.get_barrier_semaphore()
    small = [
        pltpu.make_async_copy(src, dst, loc_sem.at[k])
        for k, (src, dst) in enumerate(
            (
                (ids_hbm, ids_ref), (wts_hbm, wts_ref), (gb_hbm, gb_ref), (gc_hbm, gc_ref), (ci_hbm, ci_ref),
                (taps_hbm, taps_ref),
            )
        )
    ]
    cols = pl.ds(pl.multiple_of(tp * W, W), W)
    load_x = pltpu.make_async_copy(x_hbm.at[:, cols], xcol, loc_sem.at[6])
    load_c = pltpu.make_async_copy(c_hbm.at[:, cols], ccol, loc_sem.at[7])
    load_o = pltpu.make_async_copy(op_hbm, opv, loc_sem.at[8])
    mats = (wg_hbm, wu_hbm, wd_hbm)
    ycols = pl.ds(pl.multiple_of(ym * yb, yb), yb)
    load_w = [pltpu.make_async_copy(mats[m].at[:, ycols], wx.at[ym, m], bsem_w.at[m]) for m in range(3)]
    small[0].start()
    small[1].start()
    load_x.start()
    load_c.start()

    @pl.loop(1, ns)
    def _(d):
        pl.semaphore_signal(barrier, inc=1, device_id={"sp": lax.rem(me + d, ns)}, device_id_type=MESH)

    @pl.loop(1, NX * NY)
    def _(d):
        pl.semaphore_signal(barrier, inc=1, device_id={"tp": lax.rem(tp + d, NX * NY)}, device_id_type=MESH)

    for copy in small[2:]:
        copy.start()
    for copy in load_w:
        copy.start()
    load_o.start()

    small[0].wait()
    small[1].wait()
    id0 = ids_ref[0:1, :]
    id1 = ids_ref[1:2, :]
    eio = lax.broadcasted_iota(jnp.int32, (ns, t), 0)
    oh0 = (eio == id0).astype(F32)
    oh1 = (eio == id1).astype(F32)
    before = (lax.broadcasted_iota(jnp.int32, (t, t), 0) < lax.broadcasted_iota(jnp.int32, (t, t), 1)).astype(F32).astype(BF)
    cum = dot((oh0 + oh1).astype(BF), before, 1, 0)
    slot0 = id0 * cp + jnp.sum(oh0 * cum, axis=0, keepdims=True).astype(jnp.int32)
    slot1 = id1 * cp + jnp.sum(oh1 * cum, axis=0, keepdims=True).astype(jnp.int32)
    rio = lax.broadcasted_iota(jnp.int32, (n_rows, t), 0)
    p0 = rio == slot0
    p1 = rio == slot1
    pmat = jnp.where(p0 | p1, 1.0, 0.0)
    wslot = jnp.sum(jnp.where(p0, wts_ref[0:1, :], jnp.where(p1, wts_ref[1:2, :], 0.0)), axis=1, keepdims=True)
    pb = pmat.astype(BF)
    load_x.wait()
    load_c.wait()
    picked = dot(pb, jnp.concatenate([xcol[...], ccol[...]], axis=1), 1, 0)
    disp[:, 0] = picked[:, :W].reshape(ns, cp, W).astype(BF)
    disp[:, 1] = (wslot * picked[:, W:]).reshape(ns, cp, W).astype(BF)

    for copy in small[2:]:
        copy.wait()
    mixed = gc_ref[...].astype(F32) * ci_ref[...].astype(F32)
    mhs[...] = mixed[t - 8 :, :]

    pl.semaphore_wait(barrier, ns - 1 + NX * NY - 1)

    def dispatch(j):
        k = lax.div(j, 2)
        i = lax.rem(zm - offset(k) + nz, nz) * 2 + lax.rem(j, 2)
        return rc(disp.at[i], gx.at[xm, 2 * k + core], d_s.at[j], d_r.at[2 * k + core], sp=i)

    def arrival(p):
        return rc(disp.at[p], gx.at[xm, p], d_s.at[p], d_r.at[p], sp=lax.rem(me + 1, ns))

    dispatch(1 - core).start()

    @pl.loop(2, ns)
    def _(j):
        dispatch(j).start()

    def wcopy(d, m, dst):
        block = pl.ds(pl.multiple_of(lax.rem(ym + d, NY) * yb, yb), yb)
        return rc(mats[m].at[:, block], wx.at[dst, m], wsem_s.at[d - 1, m], wsem_r.at[d - 1, m], tp=ydev(d))

    for d in (1, 3, 2):
        for m in range(3):
            go(wcopy(d, m, ym))

    halo_m = rc(mhs, mh, h_s.at[0], h_r.at[0], sp=lax.rem(me + 1, ns))
    go(halo_m)

    gx[xm, core] = disp[me]

    pt[...] = pmat.T.astype(BF)

    right, left, xfar = lax.rem(xm + 1, NX), lax.rem(xm + 3, NX), lax.rem(xm + 2, NX)
    up, down, yfar = lax.rem(ym + 1, NY), lax.rem(ym + 3, NY), lax.rem(ym + 2, NY)

    def wait_on(dst, ss, rs):
        rc(dst, dst, ss, rs, tp=xdev(1)).wait_recv()

    weights = []

    def stage_a(c):
        at, pc = STARTS[c], CHUNKS[c]
        if c == 0:
            arrival(1 - core).wait_recv()

        @pl.loop(2 if c == 0 else at, at + pc)
        def _(p):
            arrival(p).wait_recv()

        part = gx.at[xm, pl.ds(at, pc)]
        go(rc(part, part, gx_s.at[c, 0], gx_r.at[c, 0], tp=xdev(1)))
        go(rc(part, part, gx_s.at[c, 1], gx_r.at[c, 1], tp=xdev(3)))

    def stage_b(c):
        at, pc = STARTS[c], CHUNKS[c]
        wait_on(gx.at[left, pl.ds(at, pc)], gx_s.at[c, 0], gx_r.at[c, 0])
        part = gx.at[left, pl.ds(at, pc // 2)]
        go(rc(part, part, gxf_s.at[c, 0], gxf_r.at[c, 0], tp=xdev(1)))
        wait_on(gx.at[right, pl.ds(at, pc)], gx_s.at[c, 1], gx_r.at[c, 1])
        part = gx.at[right, pl.ds(at + pc // 2, pc // 2)]
        go(rc(part, part, gxf_s.at[c, 1], gxf_r.at[c, 1], tp=xdev(3)))

    def pieces(c):
        yq = CHUNKS[c] * cp // NY
        cut = -(-yq // 32) * 16
        cut = cut if c % 2 == 0 else yq - cut
        return pl.ds(0, cut), pl.ds(cut, yq - cut)

    def stage_c(c):
        at, pc = STARTS[c], CHUNKS[c]
        qr = pc * cp
        yq = qr // NY
        if c == 0:
            for m in range(3):
                load_w[m].wait()
                for d in (1, 2, 3):
                    wcopy(d, m, lax.rem(ym - d + NY, NY)).wait_recv()
            weights.extend(jnp.concatenate([wx[yy, m] for yy in range(NY)], axis=0) for m in range(3))
        wait_on(gx.at[xfar, pl.ds(at, pc // 2)], gxf_s.at[c, 0], gxf_r.at[c, 0])
        wait_on(gx.at[xfar, pl.ds(at + pc // 2, pc // 2)], gxf_s.at[c, 1], gxf_r.at[c, 1])
        for s in range(2):
            blocks = [gx[xx, at : at + pc, s].astype(F32).reshape(qr, W) for xx in range(NX)]
            rows[c][s] = jnp.concatenate(blocks, axis=1).astype(BF)
        for m in range(3):
            pre = dot(rows[c][1 if m == 2 else 0], weights[m], 1, 1)
            preb[c][:, :, m * u : (m + 1) * u] = pre.reshape(NY, yq, u).astype(BF)
        low, high = pieces(c)
        go(rc(preb[c].at[yfar, low], rs1[c].at[low], y_s.at[c, 0], y_r.at[c, 0], tp=ydev(1)))
        go(rc(preb[c].at[yfar, high], rs1[c].at[high], y_s.at[c, 1], y_r.at[c, 1], tp=ydev(3)))
        go(rc(preb[c].at[up, high], rs2[c].at[0, high], y_s.at[c, 2], y_r.at[c, 2], tp=ydev(1)))
        go(rc(preb[c].at[down, low], rs2[c].at[1, low], y_s.at[c, 3], y_r.at[c, 3], tp=ydev(3)))

    def stage_d(c):
        low, high = pieces(c)
        wait_on(rs1[c].at[low], y_s.at[c, 0], y_r.at[c, 0])
        preb[c][up, low] = (preb[c][up, low].astype(F32) + rs1[c][low].astype(F32)).astype(BF)
        go(rc(preb[c].at[up, low], rs2[c].at[0, low], y_s.at[c, 4], y_r.at[c, 4], tp=ydev(1)))
        wait_on(rs1[c].at[high], y_s.at[c, 1], y_r.at[c, 1])
        preb[c][down, high] = (preb[c][down, high].astype(F32) + rs1[c][high].astype(F32)).astype(BF)
        go(rc(preb[c].at[down, high], rs2[c].at[1, high], y_s.at[c, 5], y_r.at[c, 5], tp=ydev(3)))

    def stage_e(c):
        low, high = pieces(c)
        for k, (row, part) in enumerate(((0, high), (1, low), (0, low), (1, high))):
            wait_on(rs2[c].at[row, part], y_s.at[c, 2 + k], y_r.at[c, 2 + k])

        def total(m):
            q = slice(m * u, (m + 1) * u)
            return preb[c][ym, :, q].astype(F32) + rs2[c][0, :, q].astype(F32) + rs2[c][1, :, q].astype(F32)

        pre_gate = total(0)
        pre_up = total(1)
        back = total(2)
        sigma = jax.nn.sigmoid(pre_gate)
        active = pre_gate * sigma
        act[c][ym, :, 0:u] = (back * pre_up * sigma * (1.0 + pre_gate * (1.0 - sigma))).astype(BF)
        act[c][ym, :, u : 2 * u] = (back * active).astype(BF)
        act[c][ym, :, 2 * u :] = (active * pre_up).astype(BF)
        own = act[c].at[ym]
        go(rc(own, own, a_s.at[c, 0], a_r.at[c, 0], tp=ydev(1)))
        go(rc(own, own, a_s.at[c, 1], a_r.at[c, 1], tp=ydev(3)))

    def stage_f(c):
        low, high = pieces(c)
        wait_on(act[c].at[down], a_s.at[c, 0], a_r.at[c, 0])
        part = act[c].at[down, low]
        go(rc(part, part, af_s.at[c, 0], af_r.at[c, 0], tp=ydev(1)))
        wait_on(act[c].at[up], a_s.at[c, 1], a_r.at[c, 1])
        part = act[c].at[up, high]
        go(rc(part, part, af_s.at[c, 1], af_r.at[c, 1], tp=ydev(3)))

    def halves(c):
        xh = CHUNKS[c] * cp // 2
        return pl.ds(0, xh), pl.ds(xh, xh)

    def stage_g(c):
        qr = CHUNKS[c] * cp
        lo, hi = halves(c)
        low, high = pieces(c)
        wait_on(act[c].at[yfar, low], af_s.at[c, 0], af_r.at[c, 0])
        wait_on(act[c].at[yfar, high], af_s.at[c, 1], af_r.at[c, 1])
        part = dot(act[c][:, :, 0:u].reshape(qr, u), weights[0], 1, 0)
        part = part + dot(act[c][:, :, u : 2 * u].reshape(qr, u), weights[1], 1, 0)
        for xx in range(NX):
            slotp[c][xx] = part[:, xx * W : (xx + 1) * W].astype(BF)
        go(rc(slotp[c].at[xfar, lo], xr1[c].at[0], xs_s.at[c, 0], xs_r.at[c, 0], tp=xdev(1)))
        go(rc(slotp[c].at[xfar, hi], xr1[c].at[1], xs_s.at[c, 1], xs_r.at[c, 1], tp=xdev(3)))
        go(rc(slotp[c].at[right, hi], xr2[c].at[0, hi], xs_s.at[c, 2], xs_r.at[c, 2], tp=xdev(1)))
        go(rc(slotp[c].at[left, lo], xr2[c].at[1, lo], xs_s.at[c, 3], xs_r.at[c, 3], tp=xdev(3)))

    def stage_h(c):
        lo, hi = halves(c)
        wait_on(xr1[c].at[0], xs_s.at[c, 0], xs_r.at[c, 0])
        slotp[c][right, lo] = (slotp[c][right, lo].astype(F32) + xr1[c][0].astype(F32)).astype(BF)
        go(rc(slotp[c].at[right, lo], xr2[c].at[0, lo], xs_s.at[c, 4], xs_r.at[c, 4], tp=xdev(1)))
        wait_on(xr1[c].at[1], xs_s.at[c, 1], xs_r.at[c, 1])
        slotp[c][left, hi] = (slotp[c][left, hi].astype(F32) + xr1[c][1].astype(F32)).astype(BF)
        go(rc(slotp[c].at[left, hi], xr2[c].at[1, hi], xs_s.at[c, 5], xs_r.at[c, 5], tp=xdev(3)))

    def giveback(p):
        k = lax.div(p, 2)
        i = lax.rem(zm + offset(k) + nz, nz) * 2 + lax.rem(p, 2)
        return rc(ret.at[p], retr.at[me], r_s.at[p], r_r.at[me], sp=i)

    def stage_i(c):
        at, pc = STARTS[c], CHUNKS[c]
        lo, hi = halves(c)
        for k, (row, part) in enumerate(((0, hi), (1, lo), (0, lo), (1, hi))):
            wait_on(xr2[c].at[row, part], xs_s.at[c, 2 + k], xs_r.at[c, 2 + k])
        slot = slotp[c][xm].astype(F32) + xr2[c][0].astype(F32) + xr2[c][1].astype(F32)
        ret[at : at + pc] = slot.reshape(pc, cp, W).astype(BF)
        if c == 0:
            giveback(1 - core).start()
            retr[me] = ret[core]

        @pl.loop(2 if c == 0 else at, at + pc)
        def _(p):
            giveback(p).start()

    def gwcopy(d, dst):
        return rc(gs.at[lax.rem(ym + d, NY)], gr.at[dst], gw_s.at[d - 1], gw_r.at[d - 1], tp=ydev(d))

    def weight_gradients():
        for m in range(3):
            grad = 0.0
            for c in range(NC):
                lhs = act[c][:, :, m * u : (m + 1) * u].reshape(CHUNKS[c] * cp, u)
                grad = grad + dot(lhs, rows[c][1 if m == 2 else 0], 0, 0)
            gs[:, m] = grad.reshape(NY, 64, yb).astype(BF)
        for d in (1, 3, 2):
            go(gwcopy(d, ym))
        gr[ym] = gs[ym]

    stages = (stage_a, stage_b, stage_c, stage_d, stage_e, stage_f, stage_g, stage_h, stage_i)
    for step in range(LAG * (NC - 1) + len(stages)):
        for c in range(NC):
            k = step - LAG * c
            if 0 <= k < len(stages):
                stages[k](c)
                if c == NC - 1 and k == 6:
                    weight_gradients()

    wait_halo = rc(mhs, mh, h_s.at[0], h_r.at[0], sp=lax.rem(me + 1, ns))
    wait_halo.wait_recv()
    prev = jnp.where(me == 0, 0.0, mh[...])
    ext = jnp.concatenate([prev, mixed], axis=0)
    tap = taps_ref[...]
    conv = tap[2:3] * mixed + tap[1:2] * ext[7 : 7 + t] + tap[0:1] * ext[6 : 6 + t]
    merged = (gb_ref[...].astype(F32) * conv).astype(BF)

    @pl.loop(1, ns)
    def _(d):
        i = lax.rem(me + d, ns)
        rc(ret.at[i], retr.at[i], r_s.at[i], r_r.at[i], sp=i).wait_recv()

    back_rows = retr[...].astype(F32).reshape(n_rows, W).astype(BF)
    grad_cols = ccol[...].astype(F32) + dot(pt[...], back_rows, 1, 0)
    st[tp] = grad_cols.astype(BF)

    def stcopy(dx, dy):
        to = lax.rem(ym + dy, NY) * NX + lax.rem(xm + NX - dx, NX)
        return rc(st.at[tp], st.at[tp], st_s.at[dx, dy], st_r.at[tp], tp=to)

    for dx in ORDER:
        for dy in (1, 3, 2, 0):
            if dx or dy:
                go(stcopy(dx, dy))

    for d in (1, 2, 3):
        gwcopy(d, lax.rem(ym - d + NY, NY)).wait_recv()
    for m, out in enumerate((gg_out, gu_out, gd_out)):
        for yy in range(NY):
            out[:, yy * yb : (yy + 1) * yb] = gr[yy, m].astype(F32)
    load_o.wait()

    def pair(g):
        return rc(gpp.at[g], pr.at[g], p_s.at[g], p_r.at[g], sp=zm * 2 + 1 - core)

    def onward(z):
        return rc(gq.at[z], fr.at[zm], f_s.at[z], f_r.at[zm], sp=z * 2 + core)

    def send_sums(g):
        pair(g).wait_recv()
        for yy in range(NY):
            z = yy * NX + lax.rem(xm + ORDER[g], NX)
            gq[z] = (gpo[g, yy] + pr[g, yy].astype(F32)).astype(BF)

            @pl.when(z != zm)
            def _(z=z):
                onward(z).start()

    for g, dx in enumerate(ORDER):
        xx = lax.rem(xm + dx, NX)
        for dy in range(NY):
            if dx or dy:
                src = lax.rem(ym + dy, NY) * NX + xx
                rc(st.at[tp], st.at[src], st_s.at[dx, dy], st_r.at[src], tp=src).wait_recv()
        block = jnp.concatenate([st[yy * NX + xx] for yy in range(NY)], axis=1)
        proj = dot(block, merged, 0, 0).reshape(NY, 2, 64, W)
        proj0 = proj[:, 0]
        proj1 = proj[:, 1]
        gpo[g] = jnp.where(core == 0, proj0, proj1)
        gpp[g] = jnp.where(core == 0, proj1, proj0).astype(BF)
        pair(g).start()
        if g:
            send_sums(g - 1)

    stream = jnp.concatenate([st[j] for j in range(NX * NY)], axis=1)
    grad_merged = dot(stream, opv[...], 1, 1)
    grad_conv = grad_merged * gb_ref[...].astype(F32)
    ghs[...] = grad_conv[0:8, :]
    halo_g = rc(ghs, gh, h_s.at[1], h_r.at[1], sp=lax.rem(me + ns - 1, ns))
    halo_g.start()
    send_sums(NX - 1)
    ggb_out[...] = (grad_merged * conv).astype(BF)

    halo_g.wait_recv()
    following = jnp.where(me == ns - 1, 0.0, gh[...])
    extg = jnp.concatenate([grad_conv, following], axis=0)
    grad_mixed = tap[2:3] * grad_conv + tap[1:2] * extg[1 : 1 + t] + tap[0:1] * extg[2 : 2 + t]
    ggc_out[...] = (grad_mixed * ci_ref[...].astype(F32)).astype(BF)
    gci_out[...] = (grad_mixed * gc_ref[...].astype(F32)).astype(BF)

    dispatch(1 - core).wait_send()
    giveback(1 - core).wait_send()

    @pl.loop(2, ns)
    def _(j):
        dispatch(j).wait_send()
        giveback(j).wait_send()

    halo_g.wait_send()
    for g in range(NX):
        pair(g).wait_send()
    for copy in sends:
        copy.wait_send()

    @pl.loop(1, nz)
    def _(d):
        z = lax.rem(zm + d, nz)
        rc(gq.at[z], fr.at[z], f_s.at[z], f_r.at[z], sp=z * 2 + core).wait()

    fr[zm] = gq[zm]
    gp_out[...] = jnp.sum(fr[...].astype(F32), axis=0)


def write_out(n, *refs):
    sems = refs[-1]
    copies = [pltpu.make_async_copy(refs[k], refs[n + k], sems.at[k]) for k in range(n)]
    for copy in copies:
        copy.start()
    for copy in copies:
        copy.wait()


def on_device(
    moe_input, cotangent, route_ids, route_weights, expert_gate, expert_up, expert_down,
    out_proj, gate_b, gate_c, conv_in, taps,
):
    ns = lax.axis_size("sp")
    t, model = moe_input.shape
    cap = 2 * t * route_ids.shape[1] // ns
    cp = -(-cap // 8) * 8
    n_rows = ns * cp
    yb = model // NY
    tpn = NX * NY
    units = expert_gate.shape[2]
    sds = jax.ShapeDtypeStruct
    vmem = pl.BlockSpec(memory_space=pltpu.VMEM)
    anym = pl.BlockSpec(memory_space=pltpu.HBM)
    dma = pltpu.SemaphoreType.DMA
    V = pltpu.VMEM

    def each(buffer):
        return tuple(buffer(pc * cp) for pc in CHUNKS)

    scratch = [
        V((2, t), jnp.int32), V((2, t), F32), V((t, W), BF), V((t, W), BF), V((t, W), BF), V((3, W), F32),
        V((t, W), BF), V((t, W), BF), V((W, model), BF), V((ns, 2, cp, W), BF), V((NX, ns, 2, cp, W), BF),
        V((NY, 3, units, yb), BF),
        each(lambda r: V((2, r, yb), BF)), each(lambda r: V((NY, r // 4, 6 * W), BF)), each(lambda r: V((r // 4, 6 * W), BF)),
        each(lambda r: V((2, r // 4, 6 * W), BF)), each(lambda r: V((NY, r // 4, 6 * W), BF)), each(lambda r: V((NX, r, W), BF)),
        each(lambda r: V((2, r // 2, W), BF)), each(lambda r: V((2, r, W), BF)),
        V((ns, cp, W), BF), V((ns, cp, W), BF), V((t, n_rows), BF), V((tpn, t, W), BF),
        V((NY, 3, units, yb), BF), V((NY, 3, units, yb), BF), V((8, W), F32), V((8, W), F32), V((8, W), F32), V((8, W), F32),
        V((NX, NY, 64, W), F32), V((NX, NY, 64, W), BF), V((NX, NY, 64, W), BF), V((tpn, 64, W), BF), V((tpn, 64, W), BF),
        dma((9,)), dma((3,)), dma((3, 3)), dma((3, 3)), dma((ns,)), dma((ns,)), dma((NC, 2)), dma((NC, 2)), dma((NC, 2)), dma((NC, 2)),
        dma((NC, 6)), dma((NC, 6)), dma((NC, 2)), dma((NC, 2)), dma((NC, 2)), dma((NC, 2)),
        dma((NC, 6)), dma((NC, 6)), dma((ns,)), dma((ns,)), dma((NX, NY)), dma((tpn,)), dma((3,)), dma((3,)), dma((2,)), dma((2,)),
        dma((NX,)), dma((NX,)), dma((ns // 2,)), dma((ns // 2,)),
    ]
    out_shape = (
        sds((units, model), F32), sds((units, model), F32), sds((units, model), F32), sds((64, W), F32),
        sds((t, W), BF), sds((t, W), BF), sds((t, W), BF),
    )
    outs = pl.pallas_call(
        functools.partial(kernel, ns, cp),
        out_shape=tuple(pltpu.VMEM(o.shape, o.dtype) for o in out_shape),
        in_specs=[anym] * 12,
        out_specs=[vmem] * 7,
        scratch_shapes=scratch,
        compiler_params=pltpu.CompilerParams(collective_id=0, has_side_effects=True, vmem_limit_bytes=40 * 2**20),
    )(
        *(
            pltpu.with_memory_space_constraint(a, pltpu.HBM)
            for a in (
                route_ids.T, route_weights.T, moe_input, cotangent, expert_gate[0].T, expert_up[0].T, expert_down[0],
                out_proj, gate_b, gate_c, conv_in, taps,
            )
        )
    )
    outs = pl.pallas_call(
        functools.partial(write_out, 7),
        out_shape=tuple(pltpu.HBM(o.shape, o.dtype) for o in out_shape),
        in_specs=[vmem] * 7,
        out_specs=[anym] * 7,
        scratch_shapes=[dma((7,))],
    )(*(pltpu.with_memory_space_constraint(o, pltpu.VMEM) for o in outs))
    gg, gu, gd, gp, ggb, ggc, gci = outs
    return gg.T[None], gu.T[None], gd[None], gp.T, ggb, ggc, gci


def solution(mesh):
    row, cols = P("sp", None), P("sp", "tp")
    return jax.shard_map(
        on_device,
        mesh=mesh,
        in_specs=(
            row, row, row, row, P("sp", None, "tp"), P("sp", None, "tp"), P("sp", "tp", None), P("tp", None),
            cols, cols, cols, P(None, "tp"),
        ),
        out_specs=(
            P("sp", None, "tp"), P("sp", None, "tp"), P("sp", "tp", None), P("tp", "sp"), cols, cols, cols,
        ),
        check_vma=False,
    )
```

time: 138 us -> 114 us (0.83)
  the two profiles are of different devices: /device:TPU:1 before, /device:TPU:2 now
where the time goes in v2:
time: 114 us
  Pallas kernels  113 us (99%)
    pallas_call x1, Pallas kernels, on_device(): pl.pallas_call(functools.partial(kernel, ns, cp), out_shape=tuple((pltpu....  112 us

profile of v2, /device:TPU:2, one launch (start us, length us, event | category | flops | bytes accessed | tf_op | source)
XLA Modules:
  0.0 113.7 jit_solution(14480038454978047684)
XLA Ops:
  0.6 111.8 %shard_map.171 = (f32[64,2048]{1,0:T(8,128)S(1)}, f32[64,2048]{1,0:T(8,128)S(1)}, f32[64,2048]{1,0:T(8,128)S(1)}, f32[64,128]{1,0:T(8,128)S(1)}, bf16[176,128]{1...) custom-call(s32[2,176]{1,0:T(2,128)} %bitcast.20, f32[2,176]{1,0:T(2,128)} %bitcast.21, ...), custom_call_target="tpu_custom_call" | custom-call | tf_op jit(solution)/shard_map/pallas_call | solution.py:489
  112.4 1.2 %shard_map.172 = (f32[64,2048]{1,0:T(8,128)}, f32[64,2048]{1,0:T(8,128)}, f32[64,2048]{1,0:T(8,128)}, f32[64,128]{1,0:T(8,128)}, bf16[176,128]{1,0:T(8,128)(2,1)...) custom-call(f32[64,2048]{1,0:T(8,128)S(1)} %get-tuple-element.21.refs_0_, ...), custom_call_target="tpu_custom_call" | custom-call | tf_op jit(solution)/shard_map/pallas_call | solution.py:505

commit v3 on v2

v3 whole, which is shorter than its diff:
```python
import functools

import jax
import jax.numpy as jnp
from jax import lax
from jax.experimental import pallas as pl
from jax.experimental.pallas import tpu as pltpu
from jax.sharding import PartitionSpec as P

MESH = pl.DeviceIdType.MESH
BF = jnp.bfloat16
F32 = jnp.float32
NX = 4
NY = 4
W = 128


def dot(a, b, ca, cb):
    return lax.dot_general(a, b, (((ca,), (cb,)), ((), ())), preferred_element_type=F32)


CHUNKS = (8, 8, 8, 8)
RANGES = (0, 3, 2, 1)
NEAR = RANGES.index(0)
STARTS = tuple(sum(CHUNKS[:k]) for k in range(len(CHUNKS)))
NC = len(CHUNKS)
SEQUENCE = "a0 c0 a1 e0 a2 c1 a3 g0 c2 e1 c3 g1 e2 i0 e3 g2 i1 g3 i2 i3"
ORDER = (0, 1, 3, 2)
SENDS = (2, 1, 3)


def kernel(
    ns, cp,
    ids_hbm, wts_hbm, x_hbm, c_hbm, wg_hbm, wu_hbm, wd_hbm, op_hbm, gb_hbm, gc_hbm, ci_hbm, taps_hbm,
    gg_out, gu_out, gd_out, gp_out, ggb_out, ggc_out, gci_out,
    ids_ref, wts_ref, gb_ref, gc_ref, ci_ref, taps_ref,
    xcol, ccol, opv, disp, gx, wx, rows, preb, rs, act, hid, slotp, xr, ret, retr, pt, st,
    gs, gr, mhs, mh, ghs, gh, gpo, gpp, pr, gq, fr,
    loc_sem, bsem_w, wsem_s, wsem_r, d_s, d_r, gx_s, gx_r, y_s, y_r, a_s, a_r, hd_s, hd_r,
    xs_s, xs_r, r_s, r_r, st_s, st_r, fw_s, fw_r, gw_s, gw_r, h_s, h_r, p_s, p_r, f_s, f_r,
):
    me = lax.axis_index("sp")
    tp = lax.axis_index("tp")
    ym = lax.div(tp, NX)
    xm = lax.rem(tp, NX)
    core = lax.rem(me, 2)
    zm = lax.div(me, 2)
    nz = ns // 2
    t = ids_ref.shape[1]
    n_rows = ns * cp
    u = 2 * W
    yb = 4 * W

    def xdev(d):
        return ym * NX + lax.rem(xm + d, NX)

    def ydev(d):
        return lax.rem(ym + d, NY) * NX + xm

    def rc(src, dst, ss, rs, **where):
        return pltpu.make_async_remote_copy(
            src_ref=src, dst_ref=dst, send_sem=ss, recv_sem=rs, device_id=where, device_id_type=MESH
        )

    def offset(k):
        return lax.div(k + 1, 2) * (2 * lax.rem(k, 2) - 1)

    sends = []

    def go(copy):
        copy.start()
        sends.append(copy)

    barrier = pltpu.get_barrier_semaphore()
    small = [
        pltpu.make_async_copy(src, dst, loc_sem.at[k])
        for k, (src, dst) in enumerate(
            (
                (ids_hbm, ids_ref), (wts_hbm, wts_ref), (gb_hbm, gb_ref), (gc_hbm, gc_ref), (ci_hbm, ci_ref),
                (taps_hbm, taps_ref),
            )
        )
    ]
    cols = pl.ds(pl.multiple_of(tp * W, W), W)
    load_x = pltpu.make_async_copy(x_hbm.at[:, cols], xcol, loc_sem.at[6])
    load_c = pltpu.make_async_copy(c_hbm.at[:, cols], ccol, loc_sem.at[7])
    load_o = pltpu.make_async_copy(op_hbm, opv, loc_sem.at[8])
    mats = (wg_hbm, wu_hbm, wd_hbm)
    ycols = pl.ds(pl.multiple_of(ym * yb, yb), yb)
    load_w = [pltpu.make_async_copy(mats[m].at[:, ycols], wx.at[ym, m], bsem_w.at[m]) for m in range(3)]
    small[0].start()
    small[1].start()
    load_x.start()
    load_c.start()

    @pl.loop(1, ns)
    def _(d):
        pl.semaphore_signal(barrier, inc=1, device_id={"sp": lax.rem(me + d, ns)}, device_id_type=MESH)

    @pl.loop(1, NX * NY)
    def _(d):
        pl.semaphore_signal(barrier, inc=1, device_id={"tp": lax.rem(tp + d, NX * NY)}, device_id_type=MESH)

    for copy in small[2:]:
        copy.start()
    for copy in load_w:
        copy.start()
    load_o.start()

    small[0].wait()
    small[1].wait()
    id0 = ids_ref[0:1, :]
    id1 = ids_ref[1:2, :]
    eio = lax.broadcasted_iota(jnp.int32, (ns, t), 0)
    oh0 = (eio == id0).astype(F32)
    oh1 = (eio == id1).astype(F32)
    before = (lax.broadcasted_iota(jnp.int32, (t, t), 0) < lax.broadcasted_iota(jnp.int32, (t, t), 1)).astype(F32).astype(BF)
    cum = dot((oh0 + oh1).astype(BF), before, 1, 0)
    slot0 = id0 * cp + jnp.sum(oh0 * cum, axis=0, keepdims=True).astype(jnp.int32)
    slot1 = id1 * cp + jnp.sum(oh1 * cum, axis=0, keepdims=True).astype(jnp.int32)
    rio = lax.broadcasted_iota(jnp.int32, (n_rows, t), 0)
    p0 = rio == slot0
    p1 = rio == slot1
    pmat = jnp.where(p0 | p1, 1.0, 0.0)
    wslot = jnp.sum(jnp.where(p0, wts_ref[0:1, :], jnp.where(p1, wts_ref[1:2, :], 0.0)), axis=1, keepdims=True)
    pb = pmat.astype(BF)
    load_x.wait()
    load_c.wait()
    picked = dot(pb, jnp.concatenate([xcol[...], ccol[...]], axis=1), 1, 0)
    disp[:, 0] = picked[:, :W].reshape(ns, cp, W).astype(BF)
    disp[:, 1] = (wslot * picked[:, W:]).reshape(ns, cp, W).astype(BF)

    for copy in small[2:]:
        copy.wait()
    mixed = gc_ref[...].astype(F32) * ci_ref[...].astype(F32)
    mhs[...] = mixed[t - 8 :, :]

    pl.semaphore_wait(barrier, ns - 1 + NX * NY - 1)

    def distance(c, j):
        return offset(RANGES[c] * 4 + lax.div(j, 2))

    def dispatch(c, j):
        i = lax.rem(zm - distance(c, j) + nz, nz) * 2 + lax.rem(j, 2)
        place = STARTS[c] + j - lax.rem(j, 2) + core
        return rc(disp.at[i], gx.at[xm, place], d_s.at[STARTS[c] + j], d_r.at[place], sp=i)

    def arrival(p):
        return rc(disp.at[p], gx.at[xm, p], d_s.at[p], d_r.at[p], sp=lax.rem(me + 1, ns))

    def each_place(c, act_on):
        if c == NEAR:
            act_on(1 - core)

        @pl.loop(2 if c == NEAR else 0, CHUNKS[c])
        def _(j):
            act_on(j)

    own_place = STARTS[NEAR] + core
    for c in range(NC):
        each_place(c, lambda j, c=c: dispatch(c, j).start())

    def wcopy(d, m, dst):
        block = pl.ds(pl.multiple_of(lax.rem(ym + d, NY) * yb, yb), yb)
        return rc(mats[m].at[:, block], wx.at[dst, m], wsem_s.at[d - 1, m], wsem_r.at[d - 1, m], tp=ydev(d))

    for d in (1, 3, 2):
        for m in range(3):
            go(wcopy(d, m, ym))

    halo_m = rc(mhs, mh, h_s.at[0], h_r.at[0], sp=lax.rem(me + 1, ns))
    go(halo_m)

    gx[xm, own_place] = disp[me]

    pt[...] = pmat.T.astype(BF)

    def wait_on(dst, ss, rs):
        rc(dst, dst, ss, rs, tp=xdev(1)).wait_recv()

    weights = []

    def stage_a(c):
        at, pc = STARTS[c], CHUNKS[c]
        each_place(c, lambda j: arrival(at + j).wait_recv())
        part = gx.at[xm, pl.ds(at, pc)]
        for d in SENDS:
            go(rc(part, part, gx_s.at[c, d - 1], gx_r.at[c, d - 1], tp=xdev(d)))

    def stage_c(c):
        at, pc = STARTS[c], CHUNKS[c]
        qr = pc * cp
        yq = qr // NY
        if c == 0:
            for m in range(3):
                load_w[m].wait()
                for d in (1, 2, 3):
                    wcopy(d, m, lax.rem(ym - d + NY, NY)).wait_recv()
            weights.extend(jnp.concatenate([wx[yy, m] for yy in range(NY)], axis=0) for m in range(3))
        for d in SENDS:
            wait_on(gx.at[lax.rem(xm + NX - d, NX), pl.ds(at, pc)], gx_s.at[c, d - 1], gx_r.at[c, d - 1])
        for s in range(2):
            blocks = [gx[xx, at : at + pc, s].astype(F32).reshape(qr, W) for xx in range(NX)]
            rows[c][s] = jnp.concatenate(blocks, axis=1).astype(BF)
        for m in range(3):
            pre = dot(rows[c][1 if m == 2 else 0], weights[m], 1, 1)
            preb[c][:, :, m * u : (m + 1) * u] = pre.reshape(NY, yq, u).astype(BF)
        for d in SENDS:
            to = lax.rem(ym + d, NY)
            go(rc(preb[c].at[to], rs[c].at[d - 1], y_s.at[c, d - 1], y_r.at[c, d - 1], tp=ydev(d)))

    def stage_e(c):
        for d in SENDS:
            wait_on(rs[c].at[d - 1], y_s.at[c, d - 1], y_r.at[c, d - 1])

        def total(m):
            q = slice(m * u, (m + 1) * u)
            return preb[c][ym, :, q].astype(F32) + sum(rs[c][k, :, q].astype(F32) for k in range(3))

        pre_gate = total(0)
        pre_up = total(1)
        back = total(2)
        sigma = jax.nn.sigmoid(pre_gate)
        active = pre_gate * sigma
        act[c][ym, :, 0:u] = (back * pre_up * sigma * (1.0 + pre_gate * (1.0 - sigma))).astype(BF)
        act[c][ym, :, u : 2 * u] = (back * active).astype(BF)
        hid[c][ym] = (active * pre_up).astype(BF)
        own = act[c].at[ym]
        for d in SENDS:
            go(rc(own, own, a_s.at[c, d - 1], a_r.at[c, d - 1], tp=ydev(d)))

    def stage_g(c):
        qr = CHUNKS[c] * cp
        for d in SENDS:
            wait_on(act[c].at[lax.rem(ym + NY - d, NY)], a_s.at[c, d - 1], a_r.at[c, d - 1])
        part = dot(act[c][:, :, 0:u].reshape(qr, u), weights[0], 1, 0)
        part = part + dot(act[c][:, :, u : 2 * u].reshape(qr, u), weights[1], 1, 0)
        for xx in range(NX):
            slotp[c][xx] = part[:, xx * W : (xx + 1) * W].astype(BF)
        for d in SENDS:
            to = lax.rem(xm + d, NX)
            go(rc(slotp[c].at[to], xr[c].at[d - 1], xs_s.at[c, d - 1], xs_r.at[c, d - 1], tp=xdev(d)))

    def giveback(c, j):
        p = STARTS[c] + j
        i = lax.rem(zm + distance(c, j) + nz, nz) * 2 + lax.rem(j, 2)
        return rc(ret.at[p], retr.at[me], r_s.at[p], r_r.at[me], sp=i)

    def stage_i(c):
        at, pc = STARTS[c], CHUNKS[c]
        for d in SENDS:
            wait_on(xr[c].at[d - 1], xs_s.at[c, d - 1], xs_r.at[c, d - 1])
        slot = slotp[c][xm].astype(F32) + sum(xr[c][k].astype(F32) for k in range(3))
        ret[at : at + pc] = slot.reshape(pc, cp, W).astype(BF)
        if c == NEAR:
            retr[me] = ret[own_place]
        each_place(c, lambda j: giveback(c, j).start())

    def gwcopy(d, dst, k):
        part = pl.ds(2 * k, 2 - k)
        return rc(gs.at[lax.rem(ym + d, NY), part], gr.at[dst, part], gw_s.at[d - 1, k], gw_r.at[d - 1, k], tp=ydev(d))

    def weight_gradient(m, lefts):
        grad = 0.0
        for c in range(NC):
            left = lefts[c][:, :, m * u : (m + 1) * u] if m < 2 else lefts[c][...]
            grad = grad + dot(left.reshape(CHUNKS[c] * cp, u), rows[c][1 if m == 2 else 0], 0, 0)
        gs[:, m] = grad.reshape(NY, 64, yb).astype(BF)

    def gate_and_up():
        for c in range(NC):
            own = hid[c].at[ym]
            for d in SENDS:
                go(rc(own, own, hd_s.at[c, d - 1], hd_r.at[c, d - 1], tp=ydev(d)))
        for m in range(2):
            weight_gradient(m, act)
        for d in SENDS:
            go(gwcopy(d, ym, 0))

    def down():
        for c in range(NC):
            for d in SENDS:
                wait_on(hid[c].at[lax.rem(ym + NY - d, NY)], hd_s.at[c, d - 1], hd_r.at[c, d - 1])
        weight_gradient(2, hid)
        for d in SENDS:
            go(gwcopy(d, ym, 1))
        gr[ym] = gs[ym]

    stages = (stage_a, stage_c, stage_e, stage_g, stage_i)
    for item in SEQUENCE.split():
        k, c = "acegi".index(item[0]), int(item[1])
        stages[k](c)
        if k == 3 and c == NC - 1:
            gate_and_up()
    wait_halo = rc(mhs, mh, h_s.at[0], h_r.at[0], sp=lax.rem(me + 1, ns))
    wait_halo.wait_recv()
    prev = jnp.where(me == 0, 0.0, mh[...])
    ext = jnp.concatenate([prev, mixed], axis=0)
    tap = taps_ref[...]
    conv = tap[2:3] * mixed + tap[1:2] * ext[7 : 7 + t] + tap[0:1] * ext[6 : 6 + t]
    merged = (gb_ref[...].astype(F32) * conv).astype(BF)

    @pl.loop(1, ns)
    def _(d):
        i = lax.rem(me + d, ns)
        rc(ret.at[i], retr.at[i], r_s.at[i], r_r.at[i], sp=i).wait_recv()

    back_rows = retr[...].astype(F32).reshape(n_rows, W).astype(BF)
    grad_cols = ccol[...].astype(F32) + dot(pt[...], back_rows, 1, 0)
    st[tp] = grad_cols.astype(BF)

    cut = -(-t // 32) * 16
    first, rest = pl.ds(0, cut), pl.ds(cut, t - cut)

    for d in SENDS:
        go(rc(st.at[tp], st.at[tp], st_s.at[0, d], st_r.at[tp], tp=ydev(d)))
        go(rc(st.at[tp], st.at[tp], st_s.at[1, d], st_r.at[tp], tp=xdev(d)))
    for d in SENDS:
        src = ydev(NY - d)
        wait_on(st.at[src], st_s.at[0, d], st_r.at[src])
        for e in SENDS:
            go(rc(st.at[src, first], st.at[src, first], fw_s.at[0, d, e], fw_r.at[0, src], tp=xdev(e)))
    for d in SENDS:
        src = xdev(NX - d)
        wait_on(st.at[src], st_s.at[1, d], st_r.at[src])
        for e in SENDS:
            go(rc(st.at[src, rest], st.at[src, rest], fw_s.at[1, d, e], fw_r.at[1, src], tp=ydev(e)))

    load_o.wait()

    def pair(g):
        return rc(gpp.at[g], pr.at[g], p_s.at[g], p_r.at[g], sp=zm * 2 + 1 - core)

    def onward(z):
        return rc(gq.at[z], fr.at[zm], f_s.at[z], f_r.at[zm], sp=z * 2 + core)

    def send_sums(g):
        pair(g).wait_recv()
        for far in (2, 1, 3, 0):
            yy = lax.rem(lax.div(zm, NX) + far, NY)
            z = yy * NX + lax.rem(xm + ORDER[g], NX)
            gq[z] = (gpo[g, yy] + pr[g, yy].astype(F32)).astype(BF)

            @pl.when(z != zm)
            def _(z=z):
                onward(z).start()

    for g, dx in enumerate(ORDER):
        xx = lax.rem(xm + dx, NX)
        for dy in range(NY):
            if dx and dy:
                src = lax.rem(ym + dy, NY) * NX + xx
                wait_on(st.at[src, first], fw_s.at[0, 1, 1], fw_r.at[0, src])
                wait_on(st.at[src, rest], fw_s.at[1, 1, 1], fw_r.at[1, src])
        block = jnp.concatenate([st[yy * NX + xx] for yy in range(NY)], axis=1)
        proj = dot(block, merged, 0, 0).reshape(NY, 2, 64, W)
        proj0 = proj[:, 0]
        proj1 = proj[:, 1]
        gpo[g] = jnp.where(core == 0, proj0, proj1)
        gpp[g] = jnp.where(core == 0, proj1, proj0).astype(BF)
        pair(g).start()
        if g == 0:
            send_sums(0)
        elif g > 1:
            send_sums(g - 1)

    stream = jnp.concatenate([st[j] for j in range(NX * NY)], axis=1)
    grad_merged = dot(stream, opv[...], 1, 1)
    grad_conv = grad_merged * gb_ref[...].astype(F32)
    ghs[...] = grad_conv[0:8, :]
    halo_g = rc(ghs, gh, h_s.at[1], h_r.at[1], sp=lax.rem(me + ns - 1, ns))
    halo_g.start()
    send_sums(NX - 1)
    ggb_out[...] = (grad_merged * conv).astype(BF)
    down()

    halo_g.wait_recv()
    following = jnp.where(me == ns - 1, 0.0, gh[...])
    extg = jnp.concatenate([grad_conv, following], axis=0)
    grad_mixed = tap[2:3] * grad_conv + tap[1:2] * extg[1 : 1 + t] + tap[0:1] * extg[2 : 2 + t]
    ggc_out[...] = (grad_mixed * ci_ref[...].astype(F32)).astype(BF)
    gci_out[...] = (grad_mixed * gc_ref[...].astype(F32)).astype(BF)

    for k in range(2):
        for d in SENDS:
            gwcopy(d, lax.rem(ym - d + NY, NY), k).wait_recv()
    for m, out in enumerate((gg_out, gu_out, gd_out)):
        for yy in range(NY):
            out[:, yy * yb : (yy + 1) * yb] = gr[yy, m].astype(F32)
    for c in range(NC):
        each_place(c, lambda j, c=c: dispatch(c, j).wait_send())
        each_place(c, lambda j, c=c: giveback(c, j).wait_send())

    halo_g.wait_send()
    for g in range(NX):
        pair(g).wait_send()
    for copy in sends:
        copy.wait_send()

    @pl.loop(1, nz)
    def _(d):
        z = lax.rem(zm + d, nz)
        rc(gq.at[z], fr.at[z], f_s.at[z], f_r.at[z], sp=z * 2 + core).wait()

    fr[zm] = gq[zm]
    gp_out[...] = jnp.sum(fr[...].astype(F32), axis=0)


def write_out(n, *refs):
    sems = refs[-1]
    copies = [pltpu.make_async_copy(refs[k], refs[n + k], sems.at[k]) for k in range(n)]
    for copy in copies:
        copy.start()
    for copy in copies:
        copy.wait()


def on_device(
    moe_input, cotangent, route_ids, route_weights, expert_gate, expert_up, expert_down,
    out_proj, gate_b, gate_c, conv_in, taps,
):
    ns = lax.axis_size("sp")
    t, model = moe_input.shape
    cap = 2 * t * route_ids.shape[1] // ns
    cp = -(-cap // 8) * 8
    n_rows = ns * cp
    yb = model // NY
    tpn = NX * NY
    units = expert_gate.shape[2]
    sds = jax.ShapeDtypeStruct
    vmem = pl.BlockSpec(memory_space=pltpu.VMEM)
    anym = pl.BlockSpec(memory_space=pltpu.HBM)
    dma = pltpu.SemaphoreType.DMA
    V = pltpu.VMEM

    def each(buffer):
        return tuple(buffer(pc * cp) for pc in CHUNKS)

    scratch = [
        V((2, t), jnp.int32), V((2, t), F32), V((t, W), BF), V((t, W), BF), V((t, W), BF), V((3, W), F32),
        V((t, W), BF), V((t, W), BF), V((W, model), BF), V((ns, 2, cp, W), BF), V((NX, ns, 2, cp, W), BF),
        V((NY, 3, units, yb), BF),
        each(lambda r: V((2, r, yb), BF)), each(lambda r: V((NY, r // 4, 6 * W), BF)), each(lambda r: V((3, r // 4, 6 * W), BF)),
        each(lambda r: V((NY, r // 4, 4 * W), BF)), each(lambda r: V((NY, r // 4, 2 * W), BF)), each(lambda r: V((NX, r, W), BF)),
        each(lambda r: V((3, r, W), BF)),
        V((ns, cp, W), BF), V((ns, cp, W), BF), V((t, n_rows), BF), V((tpn, t, W), BF),
        V((NY, 3, units, yb), BF), V((NY, 3, units, yb), BF), V((8, W), F32), V((8, W), F32), V((8, W), F32), V((8, W), F32),
        V((NX, NY, 64, W), F32), V((NX, NY, 64, W), BF), V((NX, NY, 64, W), BF), V((tpn, 64, W), BF), V((tpn, 64, W), BF),
        dma((9,)), dma((3,)), dma((3, 3)), dma((3, 3)), dma((ns,)), dma((ns,)), dma((NC, 3)), dma((NC, 3)),
        dma((NC, 3)), dma((NC, 3)), dma((NC, 3)), dma((NC, 3)), dma((NC, 3)), dma((NC, 3)), dma((NC, 3)), dma((NC, 3)),
        dma((ns,)), dma((ns,)), dma((2, NX)), dma((tpn,)), dma((2, NY, NX)), dma((2, tpn)), dma((3, 2)), dma((3, 2)), dma((2,)), dma((2,)),
        dma((NX,)), dma((NX,)), dma((ns // 2,)), dma((ns // 2,)),
    ]
    out_shape = (
        sds((units, model), F32), sds((units, model), F32), sds((units, model), F32), sds((64, W), F32),
        sds((t, W), BF), sds((t, W), BF), sds((t, W), BF),
    )
    outs = pl.pallas_call(
        functools.partial(kernel, ns, cp),
        out_shape=tuple(pltpu.VMEM(o.shape, o.dtype) for o in out_shape),
        in_specs=[anym] * 12,
        out_specs=[vmem] * 7,
        scratch_shapes=scratch,
        compiler_params=pltpu.CompilerParams(collective_id=0, has_side_effects=True, vmem_limit_bytes=40 * 2**20),
    )(
        *(
            pltpu.with_memory_space_constraint(a, pltpu.HBM)
            for a in (
                route_ids.T, route_weights.T, moe_input, cotangent, expert_gate[0].T, expert_up[0].T, expert_down[0],
                out_proj, gate_b, gate_c, conv_in, taps,
            )
        )
    )
    outs = pl.pallas_call(
        functools.partial(write_out, 7),
        out_shape=tuple(pltpu.HBM(o.shape, o.dtype) for o in out_shape),
        in_specs=[vmem] * 7,
        out_specs=[anym] * 7,
        scratch_shapes=[dma((7,))],
    )(*(pltpu.with_memory_space_constraint(o, pltpu.VMEM) for o in outs))
    gg, gu, gd, gp, ggb, ggc, gci = outs
    return gg.T[None], gu.T[None], gd[None], gp.T, ggb, ggc, gci


def solution(mesh):
    row, cols = P("sp", None), P("sp", "tp")
    return jax.shard_map(
        on_device,
        mesh=mesh,
        in_specs=(
            row, row, row, row, P("sp", None, "tp"), P("sp", None, "tp"), P("sp", "tp", None), P("tp", None),
            cols, cols, cols, P(None, "tp"),
        ),
        out_specs=(
            P("sp", None, "tp"), P("sp", None, "tp"), P("sp", "tp", None), P("tp", "sp"), cols, cols, cols,
        ),
        check_vma=False,
    )
```

time: 114 us -> 100 us (0.88)
  the two profiles are of different devices: /device:TPU:2 before, /device:TPU:1 now
where the time goes in v3:
time: 100 us; the launch traced here: 99.5 us
  Pallas kernels  98.8 us (99%)
    pallas_call x1, Pallas kernels, on_device(): pl.pallas_call(functools.partial(kernel, ns, cp), out_shape=tuple((pltpu....  97.6 us

profile of v3, /device:TPU:1, one launch (start us, length us, event | category | flops | bytes accessed | tf_op | source)
XLA Modules:
  0.0 99.5 jit_solution(14782220102288244419)
XLA Ops:
  0.6 97.6 %shard_map.171 = (f32[64,2048]{1,0:T(8,128)S(1)}, f32[64,2048]{1,0:T(8,128)S(1)}, f32[64,2048]{1,0:T(8,128)S(1)}, f32[64,128]{1,0:T(8,128)S(1)}, bf16[176,128]{1...) custom-call(s32[2,176]{1,0:T(2,128)} %bitcast.20, f32[2,176]{1,0:T(2,128)} %bitcast.21, ...), custom_call_target="tpu_custom_call" | custom-call | tf_op jit(solution)/shard_map/pallas_call | solution.py:458
  98.2 1.2 %shard_map.172 = (f32[64,2048]{1,0:T(8,128)}, f32[64,2048]{1,0:T(8,128)}, f32[64,2048]{1,0:T(8,128)}, f32[64,128]{1,0:T(8,128)}, bf16[176,128]{1,0:T(8,128)(2,1)...) custom-call(f32[64,2048]{1,0:T(8,128)S(1)} %get-tuple-element.21.refs_0_, ...), custom_call_target="tpu_custom_call" | custom-call | tf_op jit(solution)/shard_map/pallas_call | solution.py:474

commit v4 on v3

--- a/solution.py
+++ b/solution.py
@@ -24,7 +24,10 @@
 NEAR = RANGES.index(0)
 STARTS = tuple(sum(CHUNKS[:k]) for k in range(len(CHUNKS)))
 NC = len(CHUNKS)
-SEQUENCE = "a0 c0 a1 e0 a2 c1 a3 g0 c2 e1 c3 g1 e2 i0 e3 g2 i1 g3 i2 i3"
+SEQUENCE = (
+    (0, 0), (1, 0), (0, 1), (2, 0), (0, 2), (1, 1), (0, 3), (3, 0), (1, 2), (2, 1),
+    (1, 3), (3, 1), (2, 2), (4, 0), (2, 3), (3, 2), (4, 1), (3, 3), (4, 2), (4, 3),
+)
 ORDER = (0, 1, 3, 2)
 SENDS = (2, 1, 3)
 
@@ -32,7 +35,8 @@
 def kernel(
     ns, cp,
     ids_hbm, wts_hbm, x_hbm, c_hbm, wg_hbm, wu_hbm, wd_hbm, op_hbm, gb_hbm, gc_hbm, ci_hbm, taps_hbm,
-    gg_out, gu_out, gd_out, gp_out, ggb_out, ggc_out, gci_out,
+    gg_any, gu_any, gd_any, gp_any, ggb_any, ggc_any, gci_any,
+    gg_out, gu_out, gd_out, gp_out, ggb_out, ggc_out, gci_out, out_sem,
     ids_ref, wts_ref, gb_ref, gc_ref, ci_ref, taps_ref,
     xcol, ccol, opv, disp, gx, wx, rows, preb, rs, act, hid, slotp, xr, ret, retr, pt, st,
     gs, gr, mhs, mh, ghs, gh, gpo, gpp, pr, gq, fr,
@@ -65,11 +69,23 @@
     def offset(k):
         return lax.div(k + 1, 2) * (2 * lax.rem(k, 2) - 1)
 
-    sends = []
+    placed = [
+        pltpu.make_async_copy(src, dst, out_sem.at[k])
+        for k, (src, dst) in enumerate(
+            (
+                (gg_out, gg_any), (gu_out, gu_any), (gd_out, gd_any), (gp_out, gp_any), (ggb_out, ggb_any),
+                (ggc_out, ggc_any), (gci_out, gci_any),
+            )
+        )
+    ]
+
+    def wait_on(buffer, sem):
+        rc(buffer, buffer, sem, sem, tp=lax.rem(tp + 1, NX * NY)).wait_recv()
+
+    sent = []
 
     def go(copy):
         copy.start()
-        sends.append(copy)
 
     barrier = pltpu.get_barrier_semaphore()
     small = [
@@ -143,10 +159,7 @@
     def dispatch(c, j):
         i = lax.rem(zm - distance(c, j) + nz, nz) * 2 + lax.rem(j, 2)
         place = STARTS[c] + j - lax.rem(j, 2) + core
-        return rc(disp.at[i], gx.at[xm, place], d_s.at[STARTS[c] + j], d_r.at[place], sp=i)
-
-    def arrival(p):
-        return rc(disp.at[p], gx.at[xm, p], d_s.at[p], d_r.at[p], sp=lax.rem(me + 1, ns))
+        return rc(disp.at[i], gx.at[xm, place], d_s, d_r.at[c], sp=i)
 
     def each_place(c, act_on):
         if c == NEAR:
@@ -162,30 +175,31 @@
 
     def wcopy(d, m, dst):
         block = pl.ds(pl.multiple_of(lax.rem(ym + d, NY) * yb, yb), yb)
-        return rc(mats[m].at[:, block], wx.at[dst, m], wsem_s.at[d - 1, m], wsem_r.at[d - 1, m], tp=ydev(d))
+        return rc(mats[m].at[:, block], wx.at[dst, m], wsem_s, wsem_r, tp=ydev(d))
 
     for d in (1, 3, 2):
         for m in range(3):
             go(wcopy(d, m, ym))
 
+    sent.append((wx.at[pl.ds(0, 3)], wsem_s))
     halo_m = rc(mhs, mh, h_s.at[0], h_r.at[0], sp=lax.rem(me + 1, ns))
-    go(halo_m)
+    halo_m.start()
+    sent.append((mhs, h_s.at[0]))
+    sent.append((disp.at[pl.ds(0, ns - 1)], d_s))
 
     gx[xm, own_place] = disp[me]
 
     pt[...] = pmat.T.astype(BF)
-
-    def wait_on(dst, ss, rs):
-        rc(dst, dst, ss, rs, tp=xdev(1)).wait_recv()
 
     weights = []
 
     def stage_a(c):
         at, pc = STARTS[c], CHUNKS[c]
-        each_place(c, lambda j: arrival(at + j).wait_recv())
+        wait_on(gx.at[xm, pl.ds(at, pc - (c == NEAR))], d_r.at[c])
         part = gx.at[xm, pl.ds(at, pc)]
         for d in SENDS:
-            go(rc(part, part, gx_s.at[c, d - 1], gx_r.at[c, d - 1], tp=xdev(d)))
+            go(rc(part, part, gx_s.at[c], gx_r.at[c], tp=xdev(d)))
+        sent.append((gx.at[pl.ds(0, 3), pl.ds(at, pc)], gx_s.at[c]))
 
     def stage_c(c):
         at, pc = STARTS[c], CHUNKS[c]
@@ -194,11 +208,9 @@
         if c == 0:
             for m in range(3):
                 load_w[m].wait()
-                for d in (1, 2, 3):
-                    wcopy(d, m, lax.rem(ym - d + NY, NY)).wait_recv()
+            wait_on(wx.at[pl.ds(0, 3)], wsem_r)
             weights.extend(jnp.concatenate([wx[yy, m] for yy in range(NY)], axis=0) for m in range(3))
-        for d in SENDS:
-            wait_on(gx.at[lax.rem(xm + NX - d, NX), pl.ds(at, pc)], gx_s.at[c, d - 1], gx_r.at[c, d - 1])
+        wait_on(gx.at[pl.ds(0, 3), pl.ds(at, pc)], gx_r.at[c])
         for s in range(2):
             blocks = [gx[xx, at : at + pc, s].astype(F32).reshape(qr, W) for xx in range(NX)]
             rows[c][s] = jnp.concatenate(blocks, axis=1).astype(BF)
@@ -207,11 +219,11 @@
             preb[c][:, :, m * u : (m + 1) * u] = pre.reshape(NY, yq, u).astype(BF)
         for d in SENDS:
             to = lax.rem(ym + d, NY)
-            go(rc(preb[c].at[to], rs[c].at[d - 1], y_s.at[c, d - 1], y_r.at[c, d - 1], tp=ydev(d)))
+            go(rc(preb[c].at[to], rs[c].at[d - 1], y_s.at[c], y_r.at[c], tp=ydev(d)))
+        sent.append((rs[c], y_s.at[c]))
 
     def stage_e(c):
-        for d in SENDS:
-            wait_on(rs[c].at[d - 1], y_s.at[c, d - 1], y_r.at[c, d - 1])
+        wait_on(rs[c], y_r.at[c])
 
         def total(m):
             q = slice(m * u, (m + 1) * u)
@@ -227,29 +239,29 @@
         hid[c][ym] = (active * pre_up).astype(BF)
         own = act[c].at[ym]
         for d in SENDS:
-            go(rc(own, own, a_s.at[c, d - 1], a_r.at[c, d - 1], tp=ydev(d)))
+            go(rc(own, own, a_s.at[c], a_r.at[c], tp=ydev(d)))
+        sent.append((act[c].at[pl.ds(0, 3)], a_s.at[c]))
 
     def stage_g(c):
         qr = CHUNKS[c] * cp
-        for d in SENDS:
-            wait_on(act[c].at[lax.rem(ym + NY - d, NY)], a_s.at[c, d - 1], a_r.at[c, d - 1])
+        wait_on(act[c].at[pl.ds(0, 3)], a_r.at[c])
         part = dot(act[c][:, :, 0:u].reshape(qr, u), weights[0], 1, 0)
         part = part + dot(act[c][:, :, u : 2 * u].reshape(qr, u), weights[1], 1, 0)
         for xx in range(NX):
             slotp[c][xx] = part[:, xx * W : (xx + 1) * W].astype(BF)
         for d in SENDS:
             to = lax.rem(xm + d, NX)
-            go(rc(slotp[c].at[to], xr[c].at[d - 1], xs_s.at[c, d - 1], xs_r.at[c, d - 1], tp=xdev(d)))
+            go(rc(slotp[c].at[to], xr[c].at[d - 1], xs_s.at[c], xs_r.at[c], tp=xdev(d)))
+        sent.append((xr[c], xs_s.at[c]))
 
     def giveback(c, j):
         p = STARTS[c] + j
         i = lax.rem(zm + distance(c, j) + nz, nz) * 2 + lax.rem(j, 2)
-        return rc(ret.at[p], retr.at[me], r_s.at[p], r_r.at[me], sp=i)
+        return rc(ret.at[p], retr.at[me], r_s, r_r, sp=i)
 
     def stage_i(c):
         at, pc = STARTS[c], CHUNKS[c]
-        for d in SENDS:
-            wait_on(xr[c].at[d - 1], xs_s.at[c, d - 1], xs_r.at[c, d - 1])
+        wait_on(xr[c], xs_r.at[c])
         slot = slotp[c][xm].astype(F32) + sum(xr[c][k].astype(F32) for k in range(3))
         ret[at : at + pc] = slot.reshape(pc, cp, W).astype(BF)
         if c == NEAR:
@@ -258,7 +270,7 @@
 
     def gwcopy(d, dst, k):
         part = pl.ds(2 * k, 2 - k)
-        return rc(gs.at[lax.rem(ym + d, NY), part], gr.at[dst, part], gw_s.at[d - 1, k], gw_r.at[d - 1, k], tp=ydev(d))
+        return rc(gs.at[lax.rem(ym + d, NY), part], gr.at[dst, part], gw_s.at[k], gw_r.at[k], tp=ydev(d))
 
     def weight_gradient(m, lefts):
         grad = 0.0
@@ -271,24 +283,25 @@
         for c in range(NC):
             own = hid[c].at[ym]
             for d in SENDS:
-                go(rc(own, own, hd_s.at[c, d - 1], hd_r.at[c, d - 1], tp=ydev(d)))
+                go(rc(own, own, hd_s.at[c], hd_r.at[c], tp=ydev(d)))
+            sent.append((hid[c].at[pl.ds(0, 3)], hd_s.at[c]))
         for m in range(2):
             weight_gradient(m, act)
         for d in SENDS:
             go(gwcopy(d, ym, 0))
+        sent.append((gs.at[pl.ds(0, 3), pl.ds(0, 2)], gw_s.at[0]))
 
     def down():
         for c in range(NC):
-            for d in SENDS:
-                wait_on(hid[c].at[lax.rem(ym + NY - d, NY)], hd_s.at[c, d - 1], hd_r.at[c, d - 1])
+            wait_on(hid[c].at[pl.ds(0, 3)], hd_r.at[c])
         weight_gradient(2, hid)
         for d in SENDS:
             go(gwcopy(d, ym, 1))
+        sent.append((gs.at[pl.ds(0, 3), pl.ds(2, 1)], gw_s.at[1]))
         gr[ym] = gs[ym]
 
     stages = (stage_a, stage_c, stage_e, stage_g, stage_i)
-    for item in SEQUENCE.split():
-        k, c = "acegi".index(item[0]), int(item[1])
+    for k, c in SEQUENCE:
         stages[k](c)
         if k == 3 and c == NC - 1:
             gate_and_up()
@@ -300,10 +313,7 @@
     conv = tap[2:3] * mixed + tap[1:2] * ext[7 : 7 + t] + tap[0:1] * ext[6 : 6 + t]
     merged = (gb_ref[...].astype(F32) * conv).astype(BF)
 
-    @pl.loop(1, ns)
-    def _(d):
-        i = lax.rem(me + d, ns)
-        rc(ret.at[i], retr.at[i], r_s.at[i], r_r.at[i], sp=i).wait_recv()
+    wait_on(retr.at[pl.ds(0, ns - 1)], r_r)
 
     back_rows = retr[...].astype(F32).reshape(n_rows, W).astype(BF)
     grad_cols = ccol[...].astype(F32) + dot(pt[...], back_rows, 1, 0)
@@ -313,18 +323,21 @@
     first, rest = pl.ds(0, cut), pl.ds(cut, t - cut)
 
     for d in SENDS:
-        go(rc(st.at[tp], st.at[tp], st_s.at[0, d], st_r.at[tp], tp=ydev(d)))
-        go(rc(st.at[tp], st.at[tp], st_s.at[1, d], st_r.at[tp], tp=xdev(d)))
+        go(rc(st.at[tp], st.at[tp], st_s, st_r.at[0, d], tp=ydev(d)))
+        go(rc(st.at[tp], st.at[tp], st_s, st_r.at[1, d], tp=xdev(d)))
+    sent.append((st.at[pl.ds(0, 6)], st_s))
     for d in SENDS:
         src = ydev(NY - d)
-        wait_on(st.at[src], st_s.at[0, d], st_r.at[src])
+        wait_on(st.at[src], st_r.at[0, d])
         for e in SENDS:
-            go(rc(st.at[src, first], st.at[src, first], fw_s.at[0, d, e], fw_r.at[0, src], tp=xdev(e)))
+            go(rc(st.at[src, first], st.at[src, first], fw_s.at[0], fw_r.at[0, e], tp=xdev(e)))
     for d in SENDS:
         src = xdev(NX - d)
-        wait_on(st.at[src], st_s.at[1, d], st_r.at[src])
+        wait_on(st.at[src], st_r.at[1, d])
         for e in SENDS:
-            go(rc(st.at[src, rest], st.at[src, rest], fw_s.at[1, d, e], fw_r.at[1, src], tp=ydev(e)))
+            go(rc(st.at[src, rest], st.at[src, rest], fw_s.at[1], fw_r.at[1, d], tp=ydev(e)))
+    sent.append((st.at[pl.ds(0, 9), first], fw_s.at[0]))
+    sent.append((st.at[pl.ds(0, 9), rest], fw_s.at[1]))
 
     load_o.wait()
 
@@ -332,7 +345,7 @@
         return rc(gpp.at[g], pr.at[g], p_s.at[g], p_r.at[g], sp=zm * 2 + 1 - core)
 
     def onward(z):
-        return rc(gq.at[z], fr.at[zm], f_s.at[z], f_r.at[zm], sp=z * 2 + core)
+        return rc(gq.at[z], fr.at[zm], f_s, f_r, sp=z * 2 + core)
 
     def send_sums(g):
         pair(g).wait_recv()
@@ -347,11 +360,9 @@
 
     for g, dx in enumerate(ORDER):
         xx = lax.rem(xm + dx, NX)
-        for dy in range(NY):
-            if dx and dy:
-                src = lax.rem(ym + dy, NY) * NX + xx
-                wait_on(st.at[src, first], fw_s.at[0, 1, 1], fw_r.at[0, src])
-                wait_on(st.at[src, rest], fw_s.at[1, 1, 1], fw_r.at[1, src])
+        if dx:
+            wait_on(st.at[pl.ds(0, 3), first], fw_r.at[0, NX - dx])
+            wait_on(st.at[pl.ds(0, 3), rest], fw_r.at[1, NX - dx])
         block = jnp.concatenate([st[yy * NX + xx] for yy in range(NY)], axis=1)
         proj = dot(block, merged, 0, 0).reshape(NY, 2, 64, W)
         proj0 = proj[:, 0]
@@ -372,6 +383,7 @@
     halo_g.start()
     send_sums(NX - 1)
     ggb_out[...] = (grad_merged * conv).astype(BF)
+    placed[4].start()
     down()
 
     halo_g.wait_recv()
@@ -380,30 +392,30 @@
     grad_mixed = tap[2:3] * grad_conv + tap[1:2] * extg[1 : 1 + t] + tap[0:1] * extg[2 : 2 + t]
     ggc_out[...] = (grad_mixed * ci_ref[...].astype(F32)).astype(BF)
     gci_out[...] = (grad_mixed * gc_ref[...].astype(F32)).astype(BF)
+    placed[5].start()
+    placed[6].start()
 
     for k in range(2):
-        for d in SENDS:
-            gwcopy(d, lax.rem(ym - d + NY, NY), k).wait_recv()
+        wait_on(gr.at[pl.ds(0, 3), pl.ds(2 * k, 2 - k)], gw_r.at[k])
     for m, out in enumerate((gg_out, gu_out, gd_out)):
         for yy in range(NY):
             out[:, yy * yb : (yy + 1) * yb] = gr[yy, m].astype(F32)
-    for c in range(NC):
-        each_place(c, lambda j, c=c: dispatch(c, j).wait_send())
-        each_place(c, lambda j, c=c: giveback(c, j).wait_send())
-
-    halo_g.wait_send()
+        placed[m].start()
+    sent.append((ret.at[pl.ds(0, ns - 1)], r_s))
+    sent.append((ghs, h_s.at[1]))
+    for buffer, sem in sent:
+        wait_on(buffer, sem)
     for g in range(NX):
         pair(g).wait_send()
-    for copy in sends:
-        copy.wait_send()
-
-    @pl.loop(1, nz)
-    def _(d):
-        z = lax.rem(zm + d, nz)
-        rc(gq.at[z], fr.at[z], f_s.at[z], f_r.at[z], sp=z * 2 + core).wait()
+
+    wait_on(gq.at[pl.ds(0, nz - 1)], f_s)
+    wait_on(fr.at[pl.ds(0, nz - 1)], f_r)
 
     fr[zm] = gq[zm]
     gp_out[...] = jnp.sum(fr[...].astype(F32), axis=0)
+    placed[3].start()
+    for copy in placed:
+        copy.wait()
 
 
 def write_out(n, *refs):
@@ -437,6 +449,8 @@
         return tuple(buffer(pc * cp) for pc in CHUNKS)
 
     scratch = [
+        V((units, model), F32), V((units, model), F32), V((units, model), F32), V((64, W), F32),
+        V((t, W), BF), V((t, W), BF), V((t, W), BF), dma((7,)),
         V((2, t), jnp.int32), V((2, t), F32), V((t, W), BF), V((t, W), BF), V((t, W), BF), V((3, W), F32),
         V((t, W), BF), V((t, W), BF), V((W, model), BF), V((ns, 2, cp, W), BF), V((NX, ns, 2, cp, W), BF),
         V((NY, 3, units, yb), BF),
@@ -446,10 +460,10 @@
         V((ns, cp, W), BF), V((ns, cp, W), BF), V((t, n_rows), BF), V((tpn, t, W), BF),
         V((NY, 3, units, yb), BF), V((NY, 3, units, yb), BF), V((8, W), F32), V((8, W), F32), V((8, W), F32), V((8, W), F32),
         V((NX, NY, 64, W), F32), V((NX, NY, 64, W), BF), V((NX, NY, 64, W), BF), V((tpn, 64, W), BF), V((tpn, 64, W), BF),
-        dma((9,)), dma((3,)), dma((3, 3)), dma((3, 3)), dma((ns,)), dma((ns,)), dma((NC, 3)), dma((NC, 3)),
-        dma((NC, 3)), dma((NC, 3)), dma((NC, 3)), dma((NC, 3)), dma((NC, 3)), dma((NC, 3)), dma((NC, 3)), dma((NC, 3)),
-        dma((ns,)), dma((ns,)), dma((2, NX)), dma((tpn,)), dma((2, NY, NX)), dma((2, tpn)), dma((3, 2)), dma((3, 2)), dma((2,)), dma((2,)),
-        dma((NX,)), dma((NX,)), dma((ns // 2,)), dma((ns // 2,)),
+        dma((9,)), dma((3,)), dma, dma, dma, dma((NC,)), dma((NC,)), dma((NC,)),
+        dma((NC,)), dma((NC,)), dma((NC,)), dma((NC,)), dma((NC,)), dma((NC,)),
+        dma((NC,)), dma((NC,)), dma, dma, dma, dma((2, NX)), dma((2,)), dma((2, NX)), dma((2,)), dma((2,)), dma((2,)), dma((2,)),
+        dma((NX,)), dma((NX,)), dma, dma,
     ]
     out_shape = (
         sds((units, model), F32), sds((units, model), F32), sds((units, model), F32), sds((64, W), F32),
@@ -459,7 +473,7 @@
         functools.partial(kernel, ns, cp),
         out_shape=tuple(pltpu.VMEM(o.shape, o.dtype) for o in out_shape),
         in_specs=[anym] * 12,
-        out_specs=[vmem] * 7,
+        out_specs=[pl.BlockSpec(memory_space=pl.ANY)] * 7,
         scratch_shapes=scratch,
         compiler_params=pltpu.CompilerParams(collective_id=0, has_side_effects=True, vmem_limit_bytes=40 * 2**20),
     )(

time: 100 us -> 97.3 us (0.973)
  Pallas kernels: 98.8 us -> 95.8 us
    pallas_call x1, Pallas kernels: 97.6 us -> 94.6 us  [on_device(): pl.pallas_call(functools.partial(kernel, ns, cp), out_shape=tuple((pltpu....]
where the time goes in v4:
time: 97.3 us; the launch traced here: 96.5 us
  Pallas kernels  95.8 us (98%)
    pallas_call x1, Pallas kernels, on_device(): pl.pallas_call(functools.partial(kernel, ns, cp), out_shape=tuple((pltpu....  94.6 us

profile of v4, /device:TPU:1, one launch (start us, length us, event | category | flops | bytes accessed | tf_op | source)
XLA Modules:
  0.0 96.5 jit_solution(11309141823638396222)
XLA Ops:
  0.6 94.6 %shard_map.171 = (f32[64,2048]{1,0:T(8,128)S(1)}, f32[64,2048]{1,0:T(8,128)S(1)}, f32[64,2048]{1,0:T(8,128)S(1)}, f32[64,128]{1,0:T(8,128)S(1)}, bf16[176,128]{1...) custom-call(s32[2,176]{1,0:T(2,128)} %bitcast.20, f32[2,176]{1,0:T(2,128)} %bitcast.21, ...), custom_call_target="tpu_custom_call" | custom-call | tf_op jit(solution)/shard_map/pallas_call | solution.py:472
  95.2 1.2 %shard_map.172 = (f32[64,2048]{1,0:T(8,128)}, f32[64,2048]{1,0:T(8,128)}, f32[64,2048]{1,0:T(8,128)}, f32[64,128]{1,0:T(8,128)}, bf16[176,128]{1,0:T(8,128)(2,1)...) custom-call(f32[64,2048]{1,0:T(8,128)S(1)} %get-tuple-element.21.refs_0_, ...), custom_call_target="tpu_custom_call" | custom-call | tf_op jit(solution)/shard_map/pallas_call | solution.py:488

commit v5 on v4

--- a/solution.py
+++ b/solution.py
@@ -105,18 +105,18 @@
     ycols = pl.ds(pl.multiple_of(ym * yb, yb), yb)
     load_w = [pltpu.make_async_copy(mats[m].at[:, ycols], wx.at[ym, m], bsem_w.at[m]) for m in range(3)]
     small[0].start()
+
+    @pl.loop(1, ns)
+    def _(d):
+        pl.semaphore_signal(barrier, inc=1, device_id={"sp": lax.rem(me + d, ns)}, device_id_type=MESH)
+
+    @pl.loop(1, NX * NY)
+    def _(d):
+        pl.semaphore_signal(barrier, inc=1, device_id={"tp": lax.rem(tp + d, NX * NY)}, device_id_type=MESH)
+
     small[1].start()
     load_x.start()
     load_c.start()
-
-    @pl.loop(1, ns)
-    def _(d):
-        pl.semaphore_signal(barrier, inc=1, device_id={"sp": lax.rem(me + d, ns)}, device_id_type=MESH)
-
-    @pl.loop(1, NX * NY)
-    def _(d):
-        pl.semaphore_signal(barrier, inc=1, device_id={"tp": lax.rem(tp + d, NX * NY)}, device_id_type=MESH)
-
     for copy in small[2:]:
         copy.start()
     for copy in load_w:
@@ -326,20 +326,22 @@
         go(rc(st.at[tp], st.at[tp], st_s, st_r.at[0, d], tp=ydev(d)))
         go(rc(st.at[tp], st.at[tp], st_s, st_r.at[1, d], tp=xdev(d)))
     sent.append((st.at[pl.ds(0, 6)], st_s))
-    for d in SENDS:
+    for d in (1, 3, 2):
         src = ydev(NY - d)
         wait_on(st.at[src], st_r.at[0, d])
         for e in SENDS:
             go(rc(st.at[src, first], st.at[src, first], fw_s.at[0], fw_r.at[0, e], tp=xdev(e)))
-    for d in SENDS:
-        src = xdev(NX - d)
-        wait_on(st.at[src], st_r.at[1, d])
-        for e in SENDS:
-            go(rc(st.at[src, rest], st.at[src, rest], fw_s.at[1], fw_r.at[1, d], tp=ydev(e)))
-    sent.append((st.at[pl.ds(0, 9), first], fw_s.at[0]))
-    sent.append((st.at[pl.ds(0, 9), rest], fw_s.at[1]))
 
     load_o.wait()
+
+    def forward_x():
+        for d in (1, 3, 2):
+            src = xdev(NX - d)
+            wait_on(st.at[src], st_r.at[1, d])
+            for e in SENDS:
+                go(rc(st.at[src, rest], st.at[src, rest], fw_s.at[1], fw_r.at[1, d], tp=ydev(e)))
+        sent.append((st.at[pl.ds(0, 9), first], fw_s.at[0]))
+        sent.append((st.at[pl.ds(0, 9), rest], fw_s.at[1]))
 
     def pair(g):
         return rc(gpp.at[g], pr.at[g], p_s.at[g], p_r.at[g], sp=zm * 2 + 1 - core)
@@ -371,6 +373,7 @@
         gpp[g] = jnp.where(core == 0, proj1, proj0).astype(BF)
         pair(g).start()
         if g == 0:
+            forward_x()
             send_sums(0)
         elif g > 1:
             send_sums(g - 1)

time: 97.3 us -> 97.3 us (level)
  no operation moved by 1% of the time
where the time goes in v5:
time: 97.3 us; the launch traced here: 96.5 us
  Pallas kernels  95.8 us (98%)
    pallas_call x1, Pallas kernels, on_device(): pl.pallas_call(functools.partial(kernel, ns, cp), out_shape=tuple((pltpu....  94.6 us

profile of v5, /device:TPU:1, one launch (start us, length us, event | category | flops | bytes accessed | tf_op | source)
XLA Modules:
  0.0 96.5 jit_solution(9565547522476857117)
XLA Ops:
  0.6 94.6 %shard_map.171 = (f32[64,2048]{1,0:T(8,128)S(1)}, f32[64,2048]{1,0:T(8,128)S(1)}, f32[64,2048]{1,0:T(8,128)S(1)}, f32[64,128]{1,0:T(8,128)S(1)}, bf16[176,128]{1...) custom-call(s32[2,176]{1,0:T(2,128)} %bitcast.20, f32[2,176]{1,0:T(2,128)} %bitcast.21, ...), custom_call_target="tpu_custom_call" | custom-call | tf_op jit(solution)/shard_map/pallas_call | solution.py:475
  95.2 1.2 %shard_map.172 = (f32[64,2048]{1,0:T(8,128)}, f32[64,2048]{1,0:T(8,128)}, f32[64,2048]{1,0:T(8,128)}, f32[64,128]{1,0:T(8,128)}, bf16[176,128]{1,0:T(8,128)(2,1)...) custom-call(f32[64,2048]{1,0:T(8,128)S(1)} %get-tuple-element.21.refs_0_, ...), custom_call_target="tpu_custom_call" | custom-call | tf_op jit(solution)/shard_map/pallas_call | solution.py:491
